TPU v7x, 32 devices: a whole 2x2x4 slice. The times are simulated.
32 devices in a mesh: ep: 8 (over z, x), tp: 4 (over y, core).
Axes of the slice: x: 2, y: 2, z: 4, core: 2. Of those that a mesh axis runs over, the one named last changes fastest.
Arguments:
- mixer_input: bfloat16 [2048, 2048], P('ep'), may hold values from -6 to 6
- mixer_gain: float32 [2048], replicated, may hold values from 0.1 to 8
- query_one: bfloat16 [2048, 512], P(None, 'tp'), may hold values from -0.1875 to 0.1875
- query_two: bfloat16 [2048, 512], P(None, 'tp'), may hold values from -0.1875 to 0.1875
- key_one: bfloat16 [2048, 256], P(None, 'tp'), may hold values from -0.1875 to 0.1875
- key_two: bfloat16 [2048, 256], P(None, 'tp'), may hold values from -0.1875 to 0.1875
- value_weight: bfloat16 [2048, 512], P(None, 'tp'), may hold values from -0.125 to 0.125
- lambdas: float32 [8], P('tp'), may hold values from 0.3 to 0.8
- head_gain: float32 [128], replicated, may hold values from 0.1 to 1.9
- output_weight: bfloat16 [1024, 2048], P('tp'), may hold values from -0.1875 to 0.1875
- expert_input: bfloat16 [4096, 2048], P(('ep', 'tp')), may hold values from -6 to 6
- expert_gain: float32 [2048], replicated, may hold values from 0.1 to 1.9
- routes: int32 [4096, 2], P(('ep', 'tp')), may hold values from 0 to 7, all different within a row; in each aligned block of 128 rows (0 to 127, 128 to 255, ...) at most 40 rows name the same one
- route_weight: float32 [4096, 2], P(('ep', 'tp')), may hold values from 0.2 to 1
- expert_gate: bfloat16 [8, 2048, 1024], P('ep', None, 'tp'), may hold values from -0.125 to 0.125
- expert_up: bfloat16 [8, 2048, 1024], P('ep', None, 'tp'), may hold values from -0.125 to 0.125
- expert_down: bfloat16 [8, 1024, 2048], P('ep', 'tp'), may hold values from -0.1875 to 0.1875
- shared_gate: bfloat16 [2048, 512], P(None, 'tp'), may hold values from -0.125 to 0.125
- shared_up: bfloat16 [2048, 512], P(None, 'tp'), may hold values from -0.125 to 0.125
- shared_down: bfloat16 [512, 2048], P('tp'), may hold values from -0.25 to 0.25
Outputs:
- mixer_output: bfloat16 [2048, 2048], P(('ep', 'tp'))
- expert_output: bfloat16 [4096, 2048], P(('ep', 'tp'))
Inputs may be any that keep to these rules, and one draw needn't show every extreme that they name: `routes`: each row names 2 different experts; in the rows of one device no expert is named by more than 40 rows, and some device names some expert exactly 40 times.
All inputs are finite; a program needn't handle non-finite values.
Results may differ from a plain program's by a relative error of at most 0.014.
The roundings to bfloat16 on the way count: a program that leaves them out, or rounds other values in their place, can miss the bound.
Values may be sent and summed in bfloat16 or wider, within the bound.
A program may use at most 128 MiB of HBM per device.

v0:
```python
import jax
import jax.numpy as jnp
from jax import lax
from jax.sharding import PartitionSpec as P

HEAD = 64


EPS = 1e-06
NEG = -1e30


def normalize(activations, scaling):
    values = activations.astype(jnp.float32)
    factor = lax.rsqrt(jnp.mean(values * values, axis=-1, keepdims=True) + EPS)
    return (values * factor * scaling).astype(jnp.bfloat16)


def unchanged(current):
    return current


def attend(running, which_half, query_pair, key_pair, value_rows, query_start, key_start):
    maxima, totals, weighted = running
    span_rows = value_rows.shape[1]
    query_pos = query_start + jnp.arange(span_rows, dtype=jnp.int32)
    key_pos = key_start + jnp.arange(span_rows, dtype=jnp.int32)
    visible = key_pos[None, :] <= query_pos[:, None]
    for map_index in range(2):
        scores = jnp.einsum(
            "kgqd,kjd->kgqj",
            query_pair[map_index],
            key_pair[map_index],
            preferred_element_type=jnp.float32,
        ) * HEAD ** (-0.5)
        scores = jnp.where(visible, scores, NEG)
        earlier = maxima[which_half, map_index]
        latest = jnp.maximum(earlier, jnp.max(scores, axis=-1))
        shrink = jnp.exp(earlier - latest)
        weights = jnp.where(visible, jnp.exp(scores - latest[..., None]), 0.0)
        totals = totals.at[which_half, map_index].set(
            totals[which_half, map_index] * shrink + jnp.sum(weights, axis=-1)
        )
        product = jnp.einsum(
            "kgqj,kjd->kgqd",
            weights.astype(jnp.bfloat16),
            value_rows,
            preferred_element_type=jnp.float32,
        )
        weighted = weighted.at[which_half, map_index].set(
            weighted[which_half, map_index] * shrink[..., None] + product
        )
        maxima = maxima.at[which_half, map_index].set(latest)
    return (maxima, totals, weighted)


def body(
    mixer_input,
    mixer_gain,
    query_one,
    query_two,
    key_one,
    key_two,
    value_weight,
    lambdas,
    head_gain,
    output_weight,
    expert_input,
    expert_gain,
    routes,
    route_weight,
    expert_gate,
    expert_up,
    expert_down,
    shared_gate,
    shared_up,
    shared_down,
):
    ep_size = lax.axis_size("ep")
    tp_size = lax.axis_size("tp")
    ep_rank = lax.axis_index("ep")
    mixer_rows = mixer_input.shape[0]
    half_rows = mixer_rows // 2
    model_width = mixer_input.shape[1]
    query_cols = query_one.shape[1]
    key_cols = key_one.shape[1]
    value_dim = head_gain.shape[0]
    local_kv = key_cols // HEAD
    local_heads = query_cols // HEAD
    group_size = local_heads // local_kv
    normed = normalize(mixer_input, mixer_gain)
    joined_weight = jnp.concatenate([query_one, query_two, key_one, key_two, value_weight], axis=1)
    projected = jnp.dot(normed, joined_weight, preferred_element_type=jnp.float32).astype(
        jnp.bfloat16
    )
    query_part = projected[:, : 2 * query_cols]
    key_values = projected[:, 2 * query_cols :]
    low_start = ep_rank * mixer_rows
    high_queries = query_part[half_rows:]
    high_start = low_start + half_rows

    def split_queries(query_rows):
        query_first = (
            query_rows[:, :query_cols]
            .reshape(half_rows, local_kv, group_size, HEAD)
            .transpose(1, 2, 0, 3)
        )
        query_second = (
            query_rows[:, query_cols:]
            .reshape(half_rows, local_kv, group_size, HEAD)
            .transpose(1, 2, 0, 3)
        )
        return (query_first, query_second)

    def heads_of(key_rows):
        return key_rows.reshape(half_rows, local_kv, HEAD).transpose(1, 0, 2)

    query_sets = (split_queries(query_part[:half_rows]), split_queries(high_queries))
    query_starts = (low_start, high_start)
    stat_shape = (2, 2, local_kv, group_size, half_rows)
    initial = (
        jnp.full(stat_shape, NEG, jnp.float32),
        jnp.zeros(stat_shape, jnp.float32),
        jnp.zeros(stat_shape + (value_dim,), jnp.float32),
    )
    arrived = lax.all_gather(key_values, "ep", axis=0, tiled=True)
    shard_count = arrived.shape[0] // mixer_rows

    def one_shard(shard_index, current):
        for key_half in range(2):
            key_block = lax.dynamic_slice_in_dim(
                arrived, shard_index * mixer_rows + key_half * half_rows, half_rows, 0
            )
            key_pair = (
                heads_of(key_block[:, :key_cols]),
                heads_of(key_block[:, key_cols : 2 * key_cols]),
            )
            value_rows = (
                key_block[:, 2 * key_cols :]
                .reshape(half_rows, local_kv, value_dim)
                .transpose(1, 0, 2)
            )
            key_start = shard_index * mixer_rows + key_half * half_rows
            for which_half in range(2):

                def update(
                    state_in,
                    chosen=which_half,
                    key_pair=key_pair,
                    value_rows=value_rows,
                    key_begin=key_start,
                ):
                    return attend(
                        state_in,
                        chosen,
                        query_sets[chosen],
                        key_pair,
                        value_rows,
                        query_starts[chosen],
                        key_begin,
                    )

                current = lax.cond(
                    key_start <= query_starts[which_half], update, unchanged, current
                )
        return current

    maxima, totals, weighted = lax.fori_loop(0, shard_count, one_shard, initial)
    mixed = weighted / totals[..., None]
    lambda_grid = lambdas.reshape(local_kv, group_size)[None, :, :, None, None]
    combined = mixed[:, 0] - lambda_grid * mixed[:, 1]
    factor = lax.rsqrt(jnp.mean(combined * combined, axis=-1, keepdims=True) + EPS)
    normed_heads = (combined * factor * head_gain).astype(jnp.bfloat16)
    head_halves = normed_heads.transpose(0, 3, 1, 2, 4).reshape(
        2, half_rows, local_heads * value_dim
    )
    high_rows = head_halves[1]
    head_rows = jnp.concatenate([head_halves[0], high_rows], axis=0)
    token_rows = expert_input.shape[0]
    normed_experts = normalize(expert_input, expert_gain)
    experts_local = expert_gate.shape[0]
    expert_count = experts_local * ep_size
    top_count = routes.shape[1]
    capacity = max(2, 5 * token_rows * top_count // (4 * expert_count))
    slot_count = expert_count * capacity
    flat_routes = routes.reshape(-1)
    onehot = (flat_routes[:, None] == jnp.arange(expert_count, dtype=jnp.int32)[None, :]).astype(
        jnp.int32
    )
    slot_place = jnp.sum((jnp.cumsum(onehot, axis=0) - onehot) * onehot, axis=1)
    slot_ids = (flat_routes * capacity + slot_place).reshape(token_rows, top_count)
    slot_match = jnp.arange(slot_count, dtype=jnp.int32)[:, None, None] == slot_ids[None, :, :]
    select = jnp.any(slot_match, axis=2).astype(jnp.bfloat16)
    outgoing = jnp.dot(select, normed_experts, preferred_element_type=jnp.float32).astype(
        jnp.bfloat16
    )
    outgoing = outgoing.reshape(ep_size, experts_local * capacity, model_width)
    received = lax.all_to_all(outgoing, "ep", split_axis=0, concat_axis=0, tiled=True)
    expert_rows, slot_rows = (
        lax.all_gather(normed_experts, "tp", axis=0, tiled=True),
        lax.all_gather(received, "tp", axis=0, tiled=True),
    )
    slot_grid = slot_rows.reshape(tp_size, ep_size, experts_local, capacity, model_width)
    gated = jnp.einsum(
        "tsecd,edf->tsecf", slot_grid, expert_gate, preferred_element_type=jnp.float32
    )
    lifted = jnp.einsum(
        "tsecd,edf->tsecf", slot_grid, expert_up, preferred_element_type=jnp.float32
    )
    routed_hidden = (jax.nn.silu(gated) * lifted).astype(jnp.bfloat16)
    shared_gated = jnp.dot(expert_rows, shared_gate, preferred_element_type=jnp.float32)
    shared_lifted = jnp.dot(expert_rows, shared_up, preferred_element_type=jnp.float32)
    shared_hidden = (jax.nn.silu(shared_gated) * shared_lifted).astype(jnp.bfloat16)
    routed_slots = ep_size * experts_local * capacity
    expert_block = token_rows + routed_slots
    mixer_sum = lax.psum_scatter(
        jnp.dot(head_rows, output_weight, preferred_element_type=jnp.float32).astype(jnp.bfloat16),
        "tp",
        scatter_dimension=0,
        tiled=True,
    )
    block_count = lax.axis_size("tp") * expert_block // expert_block
    shared_part = jnp.dot(shared_hidden, shared_down, preferred_element_type=jnp.float32).reshape(
        block_count, token_rows, model_width
    )
    routed_part = jnp.einsum(
        "tsecf,efd->tsecd", routed_hidden, expert_down, preferred_element_type=jnp.float32
    ).reshape(block_count, routed_slots, model_width)
    expert_sum = lax.psum_scatter(
        jnp.concatenate([shared_part, routed_part], axis=1)
        .reshape(lax.axis_size("tp") * expert_block, model_width)
        .astype(jnp.bfloat16),
        "tp",
        scatter_dimension=0,
        tiled=True,
    ).astype(jnp.float32)
    shared_result = expert_sum[:token_rows]
    routed_result = (
        expert_sum[token_rows:]
        .astype(jnp.bfloat16)
        .reshape(ep_size, experts_local * capacity, model_width)
    )
    returned = lax.all_to_all(routed_result, "ep", split_axis=0, concat_axis=0, tiled=True).reshape(
        slot_count, model_width
    )
    picked = returned[slot_ids].astype(jnp.float32)
    routed_total = jnp.sum(picked * route_weight[:, :, None], axis=1)
    expert_output = (routed_total + shared_result).astype(jnp.bfloat16)
    return (mixer_sum, expert_output)


def solution(mesh):
    in_specs = (
        P("ep", None),
        P(),
        P(None, "tp"),
        P(None, "tp"),
        P(None, "tp"),
        P(None, "tp"),
        P(None, "tp"),
        P("tp"),
        P(),
        P("tp", None),
        P(("ep", "tp"), None),
        P(),
        P(("ep", "tp"), None),
        P(("ep", "tp"), None),
        P("ep", None, "tp"),
        P("ep", None, "tp"),
        P("ep", "tp", None),
        P(None, "tp"),
        P(None, "tp"),
        P("tp", None),
    )
    out_specs = (P(("ep", "tp"), None), P(("ep", "tp"), None))
    return jax.shard_map(body, mesh=mesh, in_specs=in_specs, out_specs=out_specs, check_vma=False)
```

profile of v0, /device:TPU:30, one launch (start us, length us, event | category | flops | bytes accessed | tf_op | source)
XLA Modules:
  0.0 288.1 jit_solution(5628525999704825276)
XLA Ops:
  8.6 2.0 fusion.129
  12.3 1.5 convolution_convert_fusion.2
  13.9 35.0 %all_to_all.10 = bf16[8,40,2048]{2,1,0:T(8,128)(2,1)} all-to-all(bf16[8,40,2048]{2,1,0:T(8,128)(2,1)S(1)} %bitcast.447), channel_id=1, replica_groups=mesh['ep'=8,'tp'=4] {'ep'}, dimensions={0} | all-to-all | bytes 2621440 | tf_op jit(solution)/shard_map/all_to_all | solution.py:198
  49.5 5.0 %concatenate.66 = bf16[2048,512]{1,0:T(8,128)(2,1)} concatenate(bf16[2048,128]{1,0:T(8,128)(2,1)} %param.80, bf16[2048,128]{1,0:T(8,128)(2,1)} %param.81, bf16[2048,64]{1,0:T(8,128)(2,1)S(1)} %copy.133, bf16[2048,64]{1,0:T(8,128)(2,1)S(1)} %copy.134, bf16[2048,128]{1,0:T(8,128)(2,1)} %param.84), dimensions={1} | concatenate | bytes 4194304 | tf_op jit(solution)/shard_map/concatenate | solution.py:92
  54.9 2.5 convolution_convert_fusion.4
  58.4 2.5 fusion.169
  61.0 4.1 %convolution_convert_fusion.1 = bf16[512,2048]{1,0:T(8,128)(2,1)S(1)} fusion(bf16[128,2048]{1,0:T(8,128)(2,1)} %param.97, bf16[512,2048]{1,0:T(8,128)(2,1)} %all-gather.6.cloned.1.call-done, bf16[2048,128]{1,0:T(8,128)(2,1)} %param.96, f32[512,128]{1,0:T(8,128)S(1)} %fusion.169), kind=kOutput, calls=%fused_computation.213 | convolution fusion | flops 538312704 | bytes 5505024 | tf_op jit(solution)/shard_map/dot_general | solution.py:223
  65.1 24.3 %all-gather.8.cloned.1.call-done = bf16[32,40,2048]{2,1,0:T(8,128)(2,1)} async-done(((bf16[8,40,2048]{2,1,0:T(8,128)(2,1)}), bf16[32,40,2048]{2,1,0:T(8,128)(2,1)}) %all-gather.8.cloned.1.call-update) | async-done | bytes 5242896 | tf_op jit(solution)/shard_map/all_gather | solution.py:201
  89.5 5.4 %convolution_bitcast_fusion.1 = f32[4,8,1,40,256]{4,3,1,0,2:T(8,128)} fusion(bf16[4,8,40,2048]{3,2,1,0:T(8,128)(2,1)} %bitcast.454, bf16[1,2048,256]{2,1,0:T(8,128)(2,1)} %param.92), kind=kOutput, calls=%fused_computation.224 | convolution fusion | flops 1342177280 | bytes 7602176 | tf_op jit(solution)/shard_map/tsecd,edf->tsecf/dot_general | solution.py:204
  94.9 10.9 %convolution_convert_fusion = bf16[4,8,40,2048]{3,2,1,0:T(8,128)(2,1)} fusion(bf16[4,8,40,2048]{3,2,1,0:T(8,128)(2,1)} %bitcast.455, f32[4,8,1,40,256]{4,3,1,0,2:T(8,128)} %convolution_bitcast_fusion.1, bf16[1,256,2048]{2,1,0:T(8,128)(2,1)S(1)} %copy-done, bf16[1,2048,256]{2,1,0:T(8,128)(2,1)} %param.93), kind=kOutput, calls=%fused_computation.212 | convolution fusion | flops 2688942080 | bytes 13893632 | tf_op jit(solution)/shard_map/tsecf,efd->tsecd/dot_general | solution.py:226
  105.8 6.8 %pad_maximum_fusion = bf16[4,448,2048]{2,1,0:T(8,128)(2,1)} fusion(bf16[4,320,2048]{2,1,0:T(8,128)(2,1)} %bitcast.445, bf16[4,128,2048]{2,1,0:T(8,128)(2,1)S(1)} %bitcast.444), kind=kLoop, calls=%fused_computation.211 | loop fusion | flops 14680064 | bytes 14680064 | tf_op jit(solution)/shard_map/concatenate | solution.py:230
  114.1 16.5 %all-gather.4.cloned.1.call-done = bf16[2048,256]{1,0:T(8,128)(2,1)} async-done(((bf16[256,256]{1,0:T(8,128)(2,1)}), bf16[2048,256]{1,0:T(8,128)(2,1)}) %all-gather.4.cloned.1.call-update) | async-done | bytes 1048592 | tf_op jit(solution)/shard_map/all_gather | solution.py:126
  130.6 1.5 copy.139
  132.2 103.4 %while.43 = (s32[]{:T(128)}, f32[2,2,1,2,128]{4,3,2,1,0:T(2,128)S(1)}, f32[2,2,1,2,128]{4,3,2,1,0:T(2,128)S(1)}, f32[2,2,1,2,128,128]{5,4,3,2,1,0:T(8,128)S(1)},...) while((s32[]{:T(128)}, ...), condition=%wide.region_26.0_spmd, body=%wide.region_1.26_spmd.sunk | while | flops 103623184 | bytes 8866761 | solution.py:168
  132.3 5.5 %conditional.8 = ((f32[2,2,1,2,128]{4,3,2,1,0:T(2,128)S(1)}, f32[2,2,1,2,128]{4,3,2,1,0:T(2,128)S(1)}, f32[2,2,1,2,128,128]{5,4,3,2,1,0:T(8,128)S(1)})) conditional(s32[]{:T(128)} %convert_element_type.206, (f32[2,2,1,2,128]{4,3,2,1,0:T(2,128)S(1)}, f32[2,2,1,2,128]{4,3,2,1,0:T(2,128)S(1)}, f32[2,2,1,2,128,128]{5,4,3,2,1,0:T(8,128)S(1)}) %tuple.229, ...), branch_computations={%region_2.0_spmd, %region_3.7_spmd} | conditional | flops 25905920 | bytes 2153560 | solution.py:163
  133.8 1.4 fusion.1
  139.1 5.3 %conditional.10 = ((f32[2,2,1,2,128]{4,3,2,1,0:T(2,128)S(1)}, f32[2,2,1,2,128]{4,3,2,1,0:T(2,128)S(1)}, f32[2,2,1,2,128,128]{5,4,3,2,1,0:T(8,128)S(1)})) conditional(s32[]{:T(128)} %convert_element_type.204, (f32[2,2,1,2,128]{4,3,2,1,0:T(2,128)S(1)}, f32[2,2,1,2,128]{4,3,2,1,0:T(2,128)S(1)}, ...), branch_computations={%region_14.14_spmd, %region_15.19_spmd} | conditional | flops 25905920 | bytes 2153560 | solution.py:163
  140.7 1.3 fusion.61
  145.9 5.5 %conditional.8 = ((f32[2,2,1,2,128]{4,3,2,1,0:T(2,128)S(1)}, f32[2,2,1,2,128]{4,3,2,1,0:T(2,128)S(1)}, f32[2,2,1,2,128,128]{5,4,3,2,1,0:T(8,128)S(1)})) conditional(s32[]{:T(128)} %convert_element_type.206, (f32[2,2,1,2,128]{4,3,2,1,0:T(2,128)S(1)}, f32[2,2,1,2,128]{4,3,2,1,0:T(2,128)S(1)}, f32[2,2,1,2,128,128]{5,4,3,2,1,0:T(8,128)S(1)}) %tuple.229, ...), branch_computations={%region_2.0_spmd, %region_3.7_spmd} | conditional | flops 25905920 | bytes 2153560 | solution.py:163
  147.4 1.4 fusion.1
  152.7 5.3 %conditional.10 = ((f32[2,2,1,2,128]{4,3,2,1,0:T(2,128)S(1)}, f32[2,2,1,2,128]{4,3,2,1,0:T(2,128)S(1)}, f32[2,2,1,2,128,128]{5,4,3,2,1,0:T(8,128)S(1)})) conditional(s32[]{:T(128)} %convert_element_type.204, (f32[2,2,1,2,128]{4,3,2,1,0:T(2,128)S(1)}, f32[2,2,1,2,128]{4,3,2,1,0:T(2,128)S(1)}, ...), branch_computations={%region_14.14_spmd, %region_15.19_spmd} | conditional | flops 25905920 | bytes 2153560 | solution.py:163
  159.5 5.5 %conditional.8 = ((f32[2,2,1,2,128]{4,3,2,1,0:T(2,128)S(1)}, f32[2,2,1,2,128]{4,3,2,1,0:T(2,128)S(1)}, f32[2,2,1,2,128,128]{5,4,3,2,1,0:T(8,128)S(1)})) conditional(s32[]{:T(128)} %convert_element_type.206, (f32[2,2,1,2,128]{4,3,2,1,0:T(2,128)S(1)}, f32[2,2,1,2,128]{4,3,2,1,0:T(2,128)S(1)}, f32[2,2,1,2,128,128]{5,4,3,2,1,0:T(8,128)S(1)}) %tuple.229, ...), branch_computations={%region_2.0_spmd, %region_3.7_spmd} | conditional | flops 25905920 | bytes 2153560 | solution.py:163
  161.0 1.4 fusion.1
  166.3 5.3 %conditional.10 = ((f32[2,2,1,2,128]{4,3,2,1,0:T(2,128)S(1)}, f32[2,2,1,2,128]{4,3,2,1,0:T(2,128)S(1)}, f32[2,2,1,2,128,128]{5,4,3,2,1,0:T(8,128)S(1)})) conditional(s32[]{:T(128)} %convert_element_type.204, (f32[2,2,1,2,128]{4,3,2,1,0:T(2,128)S(1)}, f32[2,2,1,2,128]{4,3,2,1,0:T(2,128)S(1)}, ...), branch_computations={%region_14.14_spmd, %region_15.19_spmd} | conditional | flops 25905920 | bytes 2153560 | solution.py:163
  167.8 1.3 fusion.61
  173.0 5.5 %conditional.8 = ((f32[2,2,1,2,128]{4,3,2,1,0:T(2,128)S(1)}, f32[2,2,1,2,128]{4,3,2,1,0:T(2,128)S(1)}, f32[2,2,1,2,128,128]{5,4,3,2,1,0:T(8,128)S(1)})) conditional(s32[]{:T(128)} %convert_element_type.206, (f32[2,2,1,2,128]{4,3,2,1,0:T(2,128)S(1)}, f32[2,2,1,2,128]{4,3,2,1,0:T(2,128)S(1)}, f32[2,2,1,2,128,128]{5,4,3,2,1,0:T(8,128)S(1)}) %tuple.229, ...), branch_computations={%region_2.0_spmd, %region_3.7_spmd} | conditional | flops 25905920 | bytes 2153560 | solution.py:163
  174.6 1.4 fusion.1
  179.9 5.3 %conditional.10 = ((f32[2,2,1,2,128]{4,3,2,1,0:T(2,128)S(1)}, f32[2,2,1,2,128]{4,3,2,1,0:T(2,128)S(1)}, f32[2,2,1,2,128,128]{5,4,3,2,1,0:T(8,128)S(1)})) conditional(s32[]{:T(128)} %convert_element_type.204, (f32[2,2,1,2,128]{4,3,2,1,0:T(2,128)S(1)}, f32[2,2,1,2,128]{4,3,2,1,0:T(2,128)S(1)}, ...), branch_computations={%region_14.14_spmd, %region_15.19_spmd} | conditional | flops 25905920 | bytes 2153560 | solution.py:163
  186.6 5.5 %conditional.8 = ((f32[2,2,1,2,128]{4,3,2,1,0:T(2,128)S(1)}, f32[2,2,1,2,128]{4,3,2,1,0:T(2,128)S(1)}, f32[2,2,1,2,128,128]{5,4,3,2,1,0:T(8,128)S(1)})) conditional(s32[]{:T(128)} %convert_element_type.206, (f32[2,2,1,2,128]{4,3,2,1,0:T(2,128)S(1)}, f32[2,2,1,2,128]{4,3,2,1,0:T(2,128)S(1)}, f32[2,2,1,2,128,128]{5,4,3,2,1,0:T(8,128)S(1)}) %tuple.229, ...), branch_computations={%region_2.0_spmd, %region_3.7_spmd} | conditional | flops 25905920 | bytes 2153560 | solution.py:163
  188.2 1.4 fusion.1
  193.4 5.3 %conditional.10 = ((f32[2,2,1,2,128]{4,3,2,1,0:T(2,128)S(1)}, f32[2,2,1,2,128]{4,3,2,1,0:T(2,128)S(1)}, f32[2,2,1,2,128,128]{5,4,3,2,1,0:T(8,128)S(1)})) conditional(s32[]{:T(128)} %convert_element_type.204, (f32[2,2,1,2,128]{4,3,2,1,0:T(2,128)S(1)}, f32[2,2,1,2,128]{4,3,2,1,0:T(2,128)S(1)}, ...), branch_computations={%region_14.14_spmd, %region_15.19_spmd} | conditional | flops 25905920 | bytes 2153560 | solution.py:163
  200.2 5.5 %conditional.8 = ((f32[2,2,1,2,128]{4,3,2,1,0:T(2,128)S(1)}, f32[2,2,1,2,128]{4,3,2,1,0:T(2,128)S(1)}, f32[2,2,1,2,128,128]{5,4,3,2,1,0:T(8,128)S(1)})) conditional(s32[]{:T(128)} %convert_element_type.206, (f32[2,2,1,2,128]{4,3,2,1,0:T(2,128)S(1)}, f32[2,2,1,2,128]{4,3,2,1,0:T(2,128)S(1)}, f32[2,2,1,2,128,128]{5,4,3,2,1,0:T(8,128)S(1)}) %tuple.229, ...), branch_computations={%region_2.0_spmd, %region_3.7_spmd} | conditional | flops 25905920 | bytes 2153560 | solution.py:163
  201.8 1.4 fusion.1
  207.0 5.3 %conditional.10 = ((f32[2,2,1,2,128]{4,3,2,1,0:T(2,128)S(1)}, f32[2,2,1,2,128]{4,3,2,1,0:T(2,128)S(1)}, f32[2,2,1,2,128,128]{5,4,3,2,1,0:T(8,128)S(1)})) conditional(s32[]{:T(128)} %convert_element_type.204, (f32[2,2,1,2,128]{4,3,2,1,0:T(2,128)S(1)}, f32[2,2,1,2,128]{4,3,2,1,0:T(2,128)S(1)}, ...), branch_computations={%region_14.14_spmd, %region_15.19_spmd} | conditional | flops 25905920 | bytes 2153560 | solution.py:163
  208.6 1.3 fusion.61
  213.8 5.5 %conditional.8 = ((f32[2,2,1,2,128]{4,3,2,1,0:T(2,128)S(1)}, f32[2,2,1,2,128]{4,3,2,1,0:T(2,128)S(1)}, f32[2,2,1,2,128,128]{5,4,3,2,1,0:T(8,128)S(1)})) conditional(s32[]{:T(128)} %convert_element_type.206, (f32[2,2,1,2,128]{4,3,2,1,0:T(2,128)S(1)}, f32[2,2,1,2,128]{4,3,2,1,0:T(2,128)S(1)}, f32[2,2,1,2,128,128]{5,4,3,2,1,0:T(8,128)S(1)}) %tuple.229, ...), branch_computations={%region_2.0_spmd, %region_3.7_spmd} | conditional | flops 25905920 | bytes 2153560 | solution.py:163
  215.4 1.4 fusion.1
  220.6 5.3 %conditional.10 = ((f32[2,2,1,2,128]{4,3,2,1,0:T(2,128)S(1)}, f32[2,2,1,2,128]{4,3,2,1,0:T(2,128)S(1)}, f32[2,2,1,2,128,128]{5,4,3,2,1,0:T(8,128)S(1)})) conditional(s32[]{:T(128)} %convert_element_type.204, (f32[2,2,1,2,128]{4,3,2,1,0:T(2,128)S(1)}, f32[2,2,1,2,128]{4,3,2,1,0:T(2,128)S(1)}, ...), branch_computations={%region_14.14_spmd, %region_15.19_spmd} | conditional | flops 25905920 | bytes 2153560 | solution.py:163
  227.4 5.5 %conditional.8 = ((f32[2,2,1,2,128]{4,3,2,1,0:T(2,128)S(1)}, f32[2,2,1,2,128]{4,3,2,1,0:T(2,128)S(1)}, f32[2,2,1,2,128,128]{5,4,3,2,1,0:T(8,128)S(1)})) conditional(s32[]{:T(128)} %convert_element_type.206, (f32[2,2,1,2,128]{4,3,2,1,0:T(2,128)S(1)}, f32[2,2,1,2,128]{4,3,2,1,0:T(2,128)S(1)}, f32[2,2,1,2,128,128]{5,4,3,2,1,0:T(8,128)S(1)}) %tuple.229, ...), branch_computations={%region_2.0_spmd, %region_3.7_spmd} | conditional | flops 25905920 | bytes 2153560 | solution.py:163
  228.9 1.4 fusion.1
  235.9 2.5 slice.1056
  238.4 6.1 %all-to-all-start.1 = ((bf16[8,40,2048]{2,1,0:T(8,128)(2,1)}), bf16[8,40,2048]{2,1,0:T(8,128)(2,1)S(1)}, u32[]{:S(2)}, u32[]{:S(2)}) async-start(bf16[8,40,2048]{2,1,0:T(8,128)(2,1)} %bitcast.446), calls=%async_computation.3 | async-start | bytes 2621440 | tf_op jit(solution)/shard_map/all_to_all | solution.py:243
  245.8 1.5 convolution_convert_fusion.3
  247.6 24.1 %all-to-all-done.1 = bf16[8,40,2048]{2,1,0:T(8,128)(2,1)S(1)} async-done(((bf16[8,40,2048]{2,1,0:T(8,128)(2,1)}), bf16[8,40,2048]{2,1,0:T(8,128)(2,1)S(1)}, u32[]{:S(2)}, u32[]{:S(2)}) %all-to-all-start.1) | async-done | bytes 1310752 | tf_op jit(solution)/shard_map/all_to_all | solution.py:243
  271.7 2.3 gather_fusion
  274.0 2.4 reshape.1975
  276.4 3.2 %multiply_reduce_fusion = f32[128,2048]{1,0:T(8,128)S(1)} fusion(f32[128,2,2048]{2,1,0:T(2,128)S(1)} %reshape.1975, f32[128,2]{1,0:T(8,128)S(1)} %copy.147), kind=kLoop, calls=%fused_computation.221 | loop fusion | flops 786432 | bytes 3146752 | tf_op jit(solution)/shard_map/reduce_sum | solution.py:247
  279.6 2.0 add_convert_fusion
  (655 shorter events, 113.7 us)
Async XLA Ops:
  7.2 87.7 %copy-start = (bf16[1,256,2048]{2,1,0:T(8,128)(2,1)S(1)}, bf16[1,256,2048]{2,1,0:T(8,128)(2,1)}, u32[]{:S(2)}) copy-start(bf16[1,256,2048]{2,1,0:T(8,128)(2,1)} %param.94) | copy-start | bytes 3145732
  7.2 3.5 %copy-start.8 = (s32[128,2]{0,1:T(2,128)S(1)}, s32[128,2]{0,1:T(2,128)}, u32[]{:S(2)}) copy-start(s32[128,2]{0,1:T(2,128)} %param.90) | copy-start | bytes 3076
  7.2 51.2 %all-gather.6.cloned.1.call-start = ((), (), s32[]{:S(2)}) async-start(), calls=%async_computation.6 | async-start | bytes 2621440 | tf_op jit(solution)/shard_map/all_gather | solution.py:200
  10.6 78.8 %all-gather.8.cloned.1.call-start = ((), (), s32[]{:S(2)}) async-start(), calls=%async_computation.7 | async-start | bytes 6553600 | tf_op jit(solution)/shard_map/all_gather | solution.py:201
  13.8 35.1 %copy-start.4 = (bf16[2048,64]{0,1:T(8,128)(2,1)S(1)}, bf16[2048,64]{0,1:T(8,128)(2,1)}, u32[]{:S(2)}) copy-start(bf16[2048,64]{0,1:T(8,128)(2,1)} %param.82) | copy-start | bytes 786436
  13.8 35.4 %copy-start.5 = (bf16[2048,64]{0,1:T(8,128)(2,1)S(1)}, bf16[2048,64]{0,1:T(8,128)(2,1)}, u32[]{:S(2)}) copy-start(bf16[2048,64]{0,1:T(8,128)(2,1)} %param.83) | copy-start | bytes 786436
  48.9 81.7 %all-gather.4.cloned.1.call-start = ((), (), s32[]{:S(2)}) async-start(), calls=%async_computation.4 | async-start | bytes 1179648 | tf_op jit(solution)/shard_map/all_gather | solution.py:126
  49.5 5.0 %copy-start.1 = (bf16[256,2048]{1,0:T(8,128)(2,1)S(1)}, bf16[256,2048]{1,0:T(8,128)(2,1)}, u32[]{:S(2)}) copy-start(bf16[256,2048]{1,0:T(8,128)(2,1)} %param.78) | copy-start | bytes 3145732
  49.5 5.3 %copy-start.12 = (f32[2048]{0:T(1024)S(1)}, f32[2048]{0:T(1024)}, u32[]{:S(2)}) copy-start(f32[2048]{0:T(1024)} %param.79) | copy-start | bytes 24580
  54.9 3.6 %copy-start.3 = (bf16[2048,128]{1,0:T(8,128)(2,1)S(1)}, bf16[2048,128]{1,0:T(8,128)(2,1)}, u32[]{:S(2)}) copy-start(bf16[2048,128]{1,0:T(8,128)(2,1)} %param.95) | copy-start | bytes 1572868
  57.4 1.0 copy-start.6
  58.2 177.7 %reduce-scatter.5.cloned.1.call-start = ((), (), s32[]{:S(2)}) async-start(), calls=%async_computation.8 | async-start | bytes 9175040 | tf_op jit(solution)/shard_map/reduce_scatter | solution.py:229
  112.6 0.9 copy-start.7
  235.8 8.7 %copy-start.9 = (f32[2]{0:T(128)S(1)}, f32[2]{0:T(128)}, u32[]{:S(2)}) copy-start(f32[2]{0:T(128)} %param.85) | copy-start | bytes 28
  238.4 6.3 %copy-start.11 = (f32[128]{0:T(128)S(1)}, f32[128]{0:T(128)}, u32[]{:S(2)}) copy-start(f32[128]{0:T(128)} %param.86) | copy-start | bytes 1540
  238.4 33.3 %all-to-all-start.1 = ((bf16[8,40,2048]{2,1,0:T(8,128)(2,1)}), bf16[8,40,2048]{2,1,0:T(8,128)(2,1)S(1)}, u32[]{:S(2)}, u32[]{:S(2)}) async-start(bf16[8,40,2048]{2,1,0:T(8,128)(2,1)} %bitcast.446), calls=%async_computation.3 | async-start | bytes 2621440 | tf_op jit(solution)/shard_map/all_to_all | solution.py:243
  244.5 37.0 %reduce-scatter.3.cloned.1.call-start = ((), (), s32[]{:S(2)}) async-start(), calls=%async_computation.5 | async-start | bytes 1310720 | tf_op jit(solution)/shard_map/reduce_scatter | solution.py:216
  244.5 1.2 copy-start.2
  244.7 2.8 copy-start.10
Sparse Core Ops, SparseCore 0:
  10.7 22.5 all-gather.5
  49.0 40.3 all-gather.7
  91.6 38.9 all-gather.3
  133.0 65.9 reduce-scatter.4
  248.1 24.7 reduce-scatter.2
where the time goes:
time: 293 us; the launch traced here: 288 us
  matrix products  73.5 us (25%)
  waiting for transfers between devices  65 us (22%)
  local copies, waits for them, and re-layouts  46.1 us (16%)
  other arithmetic  44.1 us (15%)
  blocking collectives  35 us (12%)
  between operations  14.2 us (5%)
  starting transfers between devices  6.48 us (2%)
  loops' own time  3.72 us (1%)
    all_to_all x1, blocking collectives, body(): lax.all_to_all(outgoing, 'ep', split_axis=0, concat_axis=0, tiled=True)  35 us
    dot_general x62, matrix products, attend(): jnp.einsum('kgqj,kjd->kgqd', weights.astype(jnp.bfloat16), value_rows, pr...  30.7 us
    all_gather x1, waiting for transfers between devices, body(): lax.all_gather(received, 'tp', axis=0, tiled=True)  24.3 us
    all_to_all x1, waiting for transfers between devices, body(): lax.all_to_all(routed_result, 'ep', split_axis=0, concat_axis=0, tiled=True)  24.1 us
    add x15, other arithmetic, attend(): totals[which_half, map_index] * shrink + jnp.sum(weights, axis=-1)  17.7 us
    scatter x15, local copies, waits for them, and re-layouts, attend(): totals.at[which_half, map_index]  17.6 us
    all_gather x1, waiting for transfers between devices, body(): arrived = lax.all_gather(key_values, 'ep', axis=0, tiled=True)  16.5 us
    dot_general x62, matrix products, attend(): jnp.einsum('kgqd,kjd->kgqj', query_pair[map_index], key_pair[map_index],...  14.3 us
  transfers between devices with their start and end apart: 6, of which 3 were waited for; matrix products, arithmetic and copies ran while one was open for 54% of the time, Pallas kernels for 0%

commit v1 on v0

v1 whole, which is shorter than its diff:
```python
import functools
import math

import jax
import jax.numpy as jnp
from jax import lax
from jax.experimental import pallas as pl
from jax.experimental.pallas import tpu as pltpu
from jax.sharding import PartitionSpec as P

HEAD = 64


EPS = 1e-06
NEG = -1e30
GROUPS = 4


def normalize(activations, scaling):
    values = activations.astype(jnp.float32)
    factor = lax.rsqrt(jnp.mean(values * values, axis=-1, keepdims=True) + EPS)
    return (values * factor * scaling).astype(jnp.bfloat16)


def attention_kernel(
    shape, rank_ref, lambdas_ref, queries_ref, keys_ref, gain_ref, out_ref, maxima, totals, weighted
):
    rows, chunk, local_kv, group, value_dim = shape
    rank = rank_ref[0]
    maxima[...] = jnp.full(maxima.shape, NEG, jnp.float32)
    totals[...] = jnp.zeros(totals.shape, jnp.float32)
    weighted[...] = jnp.zeros(weighted.shape, jnp.float32)
    heads = local_kv * group
    key_cols = local_kv * HEAD
    chunks = rows // chunk
    scale = HEAD**-0.5 * math.log2(math.e)

    def block(index, masked):
        start = pl.multiple_of(index * rows, rows)
        for kv in range(local_kv):
            value_start = 2 * key_cols + kv * value_dim
            for part in range(chunks):
                span = (part + 1) * chunk if masked else rows
                values = keys_ref[pl.ds(start, span), value_start : value_start + value_dim]
                for which in range(2):
                    first = which * key_cols + kv * HEAD
                    keys = keys_ref[pl.ds(start, span), first : first + HEAD]
                    for g in range(group):
                        head = kv * group + g
                        col = (which * heads + head) * HEAD
                        queries = queries_ref[part * chunk : (part + 1) * chunk, col : col + HEAD]
                        scores = lax.dot_general(
                            queries,
                            keys,
                            (((1,), (1,)), ((), ())),
                            preferred_element_type=jnp.float32,
                        )
                        if masked:
                            row = part * chunk + lax.broadcasted_iota(jnp.int32, scores.shape, 0)
                            col_pos = lax.broadcasted_iota(jnp.int32, scores.shape, 1)
                            scores = jnp.where(col_pos <= row, scores, NEG)
                        slot = (which * heads + head) * chunks + part
                        earlier = maxima[slot]
                        latest = jnp.maximum(earlier, jnp.max(scores, axis=1, keepdims=True))
                        shrink = jnp.exp2((earlier - latest) * scale)
                        weights = jnp.exp2((scores - latest[:, :1]) * scale)
                        totals[slot] = totals[slot] * shrink + jnp.sum(
                            weights, axis=1, keepdims=True
                        )
                        weighted[slot] = weighted[slot] * shrink[:, :1] + jnp.dot(
                            weights.astype(jnp.bfloat16),
                            values,
                            preferred_element_type=jnp.float32,
                        )
                        maxima[slot] = latest

    def earlier_block(index, carry):
        block(index, False)
        return carry

    lax.fori_loop(0, rank, earlier_block, 0)
    block(rank, True)
    for head in range(heads):
        for part in range(chunks):
            one = head * chunks + part
            two = (heads + head) * chunks + part
            combined = (
                weighted[one] / totals[one][:, :1]
                - lambdas_ref[head] * (weighted[two] / totals[two][:, :1])
            )
            factor = lax.rsqrt(jnp.mean(combined * combined, axis=1, keepdims=True) + EPS)
            out_ref[
                part * chunk : (part + 1) * chunk, head * value_dim : (head + 1) * value_dim
            ] = (combined * factor * gain_ref[...]).astype(jnp.bfloat16)


def attention(queries, keys, rank, lambdas, head_gain, local_kv, group):
    rows = queries.shape[0]
    value_dim = head_gain.shape[0]
    heads = local_kv * group
    chunk = min(128, rows)
    slots = 2 * heads * (rows // chunk)
    vmem = pl.BlockSpec(memory_space=pltpu.VMEM)
    smem = pl.BlockSpec(memory_space=pltpu.SMEM)
    scores = heads * 2 * rows * keys.shape[0]
    return pl.pallas_call(
        functools.partial(attention_kernel, (rows, chunk, local_kv, group, value_dim)),
        out_shape=jax.ShapeDtypeStruct((rows, heads * value_dim), jnp.bfloat16),
        in_specs=[smem, smem, vmem, vmem, vmem],
        out_specs=vmem,
        scratch_shapes=[
            pltpu.VMEM((slots, chunk, 128), jnp.float32),
            pltpu.VMEM((slots, chunk, 128), jnp.float32),
            pltpu.VMEM((slots, chunk, value_dim), jnp.float32),
        ],
        compiler_params=pltpu.CompilerParams(vmem_limit_bytes=48 * 1024 * 1024),
        cost_estimate=pl.CostEstimate(
            flops=8 * scores * HEAD, bytes_accessed=keys.size * 2, transcendentals=scores
        ),
        name="attention",
    )(rank.reshape(1), lambdas, queries, keys, head_gain.reshape(1, value_dim))


def swap(rows, axis, size, distance):
    return lax.ppermute(rows, axis, [(i, i ^ distance) for i in range(size)])


def gather_near(block, axis, size):
    places = {0: block}
    distance = size // 2
    while distance:
        held = sorted(places)
        moved = swap(jnp.stack([places[p] for p in held]), axis, size, distance)
        places.update({p ^ distance: moved[i] for i, p in enumerate(held)})
        distance //= 2
    return jnp.stack([places[p] for p in range(size)])


def scatter_near(partials, axis, size):
    sums = {p: partials[p] for p in range(size)}
    distance = 1
    while distance < size:
        kept = [p for p in sorted(sums) if not p & distance]
        sent = jnp.stack([sums[p ^ distance].astype(jnp.bfloat16) for p in kept])
        moved = swap(sent, axis, size, distance).astype(jnp.float32)
        sums = {p: sums[p].astype(jnp.float32) + moved[i] for i, p in enumerate(kept)}
        distance *= 2
    return sums[0]


def exchange(blocks, axis, size):
    return [blocks[d] if d == 0 else swap(blocks[d], axis, size, d) for d in range(size)]


def body(
    mixer_input,
    mixer_gain,
    query_one,
    query_two,
    key_one,
    key_two,
    value_weight,
    lambdas,
    head_gain,
    output_weight,
    expert_input,
    expert_gain,
    routes,
    route_weight,
    expert_gate,
    expert_up,
    expert_down,
    shared_gate,
    shared_up,
    shared_down,
):
    ep_size = lax.axis_size("ep")
    tp_size = lax.axis_size("tp")
    ep_rank = lax.axis_index("ep")
    mixer_rows = mixer_input.shape[0]
    model_width = mixer_input.shape[1]
    query_cols = query_one.shape[1]
    key_cols = key_one.shape[1]
    value_dim = head_gain.shape[0]
    local_kv = key_cols // HEAD
    local_heads = query_cols // HEAD
    group_size = local_heads // local_kv
    normed = normalize(mixer_input, mixer_gain)
    joined_weight = jnp.concatenate([query_one, query_two, key_one, key_two, value_weight], axis=1)
    projected = jnp.dot(normed, joined_weight, preferred_element_type=jnp.float32).astype(
        jnp.bfloat16
    )
    query_part = projected[:, : 2 * query_cols]
    key_values = projected[:, 2 * query_cols :]
    arrived = lax.all_gather(key_values, "ep", axis=0, tiled=True)
    head_rows = attention(
        query_part, arrived, ep_rank, lambdas, head_gain, local_kv, group_size
    )
    mixer_partial = jnp.dot(head_rows, output_weight, preferred_element_type=jnp.float32).astype(
        jnp.bfloat16
    )
    tp_rank = lax.axis_index("tp")
    own_rows = mixer_rows // tp_size
    mixer_blocks = mixer_partial.reshape(tp_size, own_rows, model_width)
    mixer_sum = scatter_near(
        [
            lax.dynamic_index_in_dim(mixer_blocks, tp_rank ^ place, 0, keepdims=False)
            for place in range(tp_size)
        ],
        "tp",
        tp_size,
    ).astype(jnp.bfloat16)

    token_rows = expert_input.shape[0]
    normed_experts = normalize(expert_input, expert_gain)
    experts_local = expert_gate.shape[0]
    expert_count = experts_local * ep_size
    top_count = routes.shape[1]
    capacity = max(2, 5 * token_rows * top_count // (4 * expert_count))
    slot_count = expert_count * capacity
    direct = ep_size <= 16
    flat_routes = routes.reshape(-1)
    if direct:
        flat_routes = ((flat_routes // experts_local) ^ ep_rank) * experts_local + (
            flat_routes % experts_local
        )
    onehot = (flat_routes[:, None] == jnp.arange(expert_count, dtype=jnp.int32)[None, :]).astype(
        jnp.int32
    )
    slot_place = jnp.sum((jnp.cumsum(onehot, axis=0) - onehot) * onehot, axis=1)
    slot_ids = (flat_routes * capacity + slot_place).reshape(token_rows, top_count)
    slot_match = jnp.arange(slot_count, dtype=jnp.int32)[:, None, None] == slot_ids[None, :, :]
    select = jnp.any(slot_match, axis=2).astype(jnp.bfloat16)
    outgoing = jnp.dot(select, normed_experts, preferred_element_type=jnp.float32).astype(
        jnp.bfloat16
    )
    pair_rows = experts_local * capacity
    outgoing = outgoing.reshape(ep_size, pair_rows, model_width)
    if direct:
        received = exchange(outgoing, "ep", ep_size)
    else:
        received = list(lax.all_to_all(outgoing, "ep", split_axis=0, concat_axis=0, tiled=True))
    bundle = max(1, ep_size // GROUPS)
    expert_rows = gather_near(normed_experts, "tp", tp_size).reshape(-1, model_width)
    shared_gated = jnp.dot(expert_rows, shared_gate, preferred_element_type=jnp.float32)
    shared_lifted = jnp.dot(expert_rows, shared_up, preferred_element_type=jnp.float32)
    shared_hidden = (jax.nn.silu(shared_gated) * shared_lifted).astype(jnp.bfloat16)
    shared_part = (
        jnp.dot(shared_hidden, shared_down, preferred_element_type=jnp.float32)
        .astype(jnp.bfloat16)
        .reshape(tp_size, token_rows, model_width)
    )
    shared_result = scatter_near(shared_part, "tp", tp_size)
    results = []
    for begin in range(0, ep_size, bundle):
        held = jnp.stack(received[begin : begin + bundle])
        slot_rows = gather_near(held, "tp", tp_size).reshape(
            tp_size * bundle, experts_local, capacity, model_width
        )
        gated = jnp.einsum("secd,edf->secf", slot_rows, expert_gate, preferred_element_type=jnp.float32)
        lifted = jnp.einsum("secd,edf->secf", slot_rows, expert_up, preferred_element_type=jnp.float32)
        routed_hidden = (jax.nn.silu(gated) * lifted).astype(jnp.bfloat16)
        routed_part = (
            jnp.einsum(
                "secf,efd->secd", routed_hidden, expert_down, preferred_element_type=jnp.float32
            )
            .astype(jnp.bfloat16)
            .reshape(tp_size, bundle, pair_rows, model_width)
        )
        total = scatter_near(routed_part, "tp", tp_size).astype(jnp.bfloat16)
        results.extend(total[i] for i in range(bundle))
    if direct:
        returned = jnp.stack(exchange(results, "ep", ep_size))
    else:
        returned = lax.all_to_all(
            jnp.stack(results), "ep", split_axis=0, concat_axis=0, tiled=True
        )
    returned = returned.reshape(slot_count, model_width)
    spread = jnp.sum(
        jnp.where(
            jnp.arange(slot_count, dtype=jnp.int32)[None, None, :] == slot_ids[:, :, None],
            route_weight[:, :, None],
            0.0,
        ),
        axis=1,
    )
    upper = lax.reduce_precision(spread, 8, 7)
    lower = lax.reduce_precision(spread - upper, 8, 7)
    routed_total = jnp.dot(
        upper.astype(jnp.bfloat16), returned, preferred_element_type=jnp.float32
    ) + jnp.dot(lower.astype(jnp.bfloat16), returned, preferred_element_type=jnp.float32)
    expert_output = (routed_total + shared_result).astype(jnp.bfloat16)
    return (mixer_sum, expert_output)


def solution(mesh):
    in_specs = (
        P("ep", None),
        P(),
        P(None, "tp"),
        P(None, "tp"),
        P(None, "tp"),
        P(None, "tp"),
        P(None, "tp"),
        P("tp"),
        P(),
        P("tp", None),
        P(("ep", "tp"), None),
        P(),
        P(("ep", "tp"), None),
        P(("ep", "tp"), None),
        P("ep", None, "tp"),
        P("ep", None, "tp"),
        P("ep", "tp", None),
        P(None, "tp"),
        P(None, "tp"),
        P("tp", None),
    )
    out_specs = (P(("ep", "tp"), None), P(("ep", "tp"), None))
    return jax.shard_map(body, mesh=mesh, in_specs=in_specs, out_specs=out_specs, check_vma=False)
```

time: 293 us -> 241 us (0.82)
  the two profiles are of different devices: /device:TPU:30 before, /device:TPU:22 now
where the time goes in v1:
time: 241 us; the launch traced here: 239 us
  waiting for transfers between devices  77.7 us (32%)
  starting transfers between devices  37.6 us (16%)
  other arithmetic  35.2 us (15%)
  matrix products  32.7 us (14%)
  local copies, waits for them, and re-layouts  26.9 us (11%)
  between operations  15 us (6%)
  Pallas kernels  14.1 us (6%)
    ppermute x36, waiting for transfers between devices, swap(): return lax.ppermute(rows, axis, [(i, i ^ distance) for i in range(size)])  77.6 us
    ppermute x36, starting transfers between devices, swap(): return lax.ppermute(rows, axis, [(i, i ^ distance) for i in range(size)])  37.6 us
    dot_general x4, matrix products, body(): jnp.einsum('secf,efd->secd', routed_hidden, expert_down, preferred_elemen...  15.8 us
    pallas_call x1, Pallas kernels, attention(): pl.pallas_call(functools.partial(attention_kernel, (rows, chunk, local_kv...  14.1 us
    unnamed x91, local copies, waits for them, and re-layouts  8.95 us
    convert_element_type x6, other arithmetic, scatter_near(): sent = jnp.stack([sums[p ^ distance].astype(jnp.bfloat16) for p in kept])  7 us
    slice x5, local copies, waits for them, and re-layouts, scatter_near(): sums = {p: partials[p] for p in range(size)}  5.79 us
    convert_element_type x6, other arithmetic, scatter_near(): moved = swap(sent, axis, size, distance).astype(jnp.float32)  5.2 us
  transfers between devices with their start and end apart: 37, of which 14 were waited for; matrix products, arithmetic and copies ran while one was open for 34% of the time, Pallas kernels for 6%

profile of v1, /device:TPU:22, one launch (start us, length us, event | category | flops | bytes accessed | tf_op | source)
XLA Modules:
  0.0 239.2 jit_solution(14786589065561454875)
XLA Ops:
  9.7 1.2 fusion.9
  10.9 1.3 convolution_convert_fusion.1
  13.7 1.5 collective-permute-start.25
  15.2 2.1 collective-permute-start.16
  17.4 1.7 collective-permute-start.17
  19.1 3.4 %collective-permute-start.8 = (bf16[40,2048]{1,0:T(8,128)(2,1)}, bf16[40,2048]{1,0:T(8,128)(2,1)}, u32[]{:S(2)}, u32[]{:S(2)}) collective-permute-start(bf16[40,2048]{1,0:T(8,128)(2,1)} %get-tuple-element.11), channel_id=1, source_target_pairs={{0,8},{4,12},{8,0},{12,4},{16,24},{20,28},{24,16},{28,20},{1,9},{5... | collective-permute-start | bytes 491528 | tf_op jit(solution)/shard_map/ppermute | solution.py:125
  22.7 1.2 copy.32
  24.0 1.5 fusion.6
  25.5 5.0 %concatenate.3 = bf16[2048,512]{1,0:T(8,128)(2,1)} concatenate(bf16[2048,128]{1,0:T(8,128)(2,1)S(1)} %copy-done.32, bf16[2048,128]{1,0:T(8,128)(2,1)} %param.23, bf16[2048,64]{1,0:T(8,128)(2,1)S(1)} %copy.31, bf16[2048,64]{1,0:T(8,128)(2,1)S(1)} %copy.32, bf16[2048,128]{1,0:T(8,128)(2,1)} %param.26), dimensions={1} | concatenate | bytes 4194304 | tf_op jit(solution)/shard_map/concatenate | solution.py:189
  30.5 2.7 %convolution_convert_fusion.7 = bf16[256,512]{1,0:T(8,128)(2,1)S(1)} fusion(bf16[2048,512]{1,0:T(8,128)(2,1)} %concatenate.3, bf16[256,2048]{1,0:T(8,128)(2,1)} %param.20, f32[2048]{0:T(1024)S(1)} %copy-done.40, f32[256]{0:T(256)S(1)} %add_rsqrt_fusion), kind=kOutput, calls=%fused_computation.26 | convolution fusion | flops 539099136 | bytes 3417088 | tf_op jit(solution)/shard_map/dot_general | solution.py:190
  35.0 3.7 %collective-permute-done.25 = bf16[40,2048]{1,0:T(8,128)(2,1)} collective-permute-done((bf16[40,2048]{1,0:T(8,128)(2,1)}, bf16[40,2048]{1,0:T(8,128)(2,1)}, u32[]{:S(2)}, u32[]{:S(2)}) %collective-permute-start.25) | collective-permute-done | bytes 163872 | tf_op jit(solution)/shard_map/ppermute | solution.py:125
  38.7 1.7 collective-permute-start.2
  42.1 1.4 collective-permute-start.26
  47.7 1.5 collective-permute-start.3
  49.2 14.0 %collective-permute-done.26 = bf16[1,2,40,2048]{3,2,1,0:T(8,128)(2,1)S(1)} collective-permute-done((bf16[1,2,40,2048]{3,2,1,0:T(8,128)(2,1)S(1)}, bf16[1,2,40,2048]{3,2,1,0:T(8,128)(2,1)S(1)}, u32[]{:S(2)}, u32[]{:S(2)}) %collective-permute-start.26) | collective-permute-done | bytes 327712 | tf_op jit(solution)/shard_map/ppermute | solution.py:125
  63.4 6.9 %collective-permute-done.18 = bf16[1,2,40,2048]{3,2,1,0:T(8,128)(2,1)S(1)} collective-permute-done((bf16[1,2,40,2048]{3,2,1,0:T(8,128)(2,1)S(1)}, bf16[1,2,40,2048]{3,2,1,0:T(8,128)(2,1)S(1)}, u32[]{:S(2)}, u32[]{:S(2)}) %collective-permute-start.18) | collective-permute-done | bytes 327712 | tf_op jit(solution)/shard_map/ppermute | solution.py:125
  71.2 5.5 %collective-permute-done.10 = bf16[1,2,40,2048]{3,2,1,0:T(8,128)(2,1)S(1)} collective-permute-done((bf16[1,2,40,2048]{3,2,1,0:T(8,128)(2,1)S(1)}, bf16[1,2,40,2048]{3,2,1,0:T(8,128)(2,1)S(1)}, u32[]{:S(2)}, u32[]{:S(2)}) %collective-permute-start.10) | collective-permute-done | bytes 327712 | tf_op jit(solution)/shard_map/ppermute | solution.py:125
  77.7 2.5 %collective-permute-done.3 = bf16[1,2,40,2048]{3,2,1,0:T(8,128)(2,1)S(1)} collective-permute-done((bf16[1,2,40,2048]{3,2,1,0:T(8,128)(2,1)S(1)}, bf16[1,2,40,2048]{3,2,1,0:T(8,128)(2,1)S(1)}, u32[]{:S(2)}, u32[]{:S(2)}) %collective-permute-start.3) | collective-permute-done | bytes 327712 | tf_op jit(solution)/shard_map/ppermute | solution.py:125
  84.3 1.3 convolution_bitcast_fusion
  85.5 3.9 %fusion.3 = bf16[8,1,40,2048]{3,2,0,1:T(8,128)(2,1)} fusion(bf16[1,256,2048]{2,1,0:T(8,128)(2,1)S(1)} %copy-done, f32[8,1,40,256]{3,2,0,1:T(8,128)} %convolution_bitcast_fusion, bf16[8,40,2048]{2,1,0:T(8,128)(2,1)S(1)} %bitcast.357, bf16[1,2048,256]{2,1,0:T(8,128)(2,1)} %param.34), kind=kOutput, calls=%fused_computation.12 | convolution fusion | flops 672235520 | bytes 5046272 | tf_op jit(solution)/shard_map/secf,efd->secd/dot_general | solution.py:264
  92.9 1.3 convolution_bitcast_fusion.2
  94.1 4.0 %fusion.2 = bf16[8,1,40,2048]{3,2,0,1:T(8,128)(2,1)} fusion(bf16[1,256,2048]{2,1,0:T(8,128)(2,1)S(1)} %copy-done, f32[8,1,40,256]{3,2,0,1:T(8,128)} %convolution_bitcast_fusion.2, bf16[8,40,2048]{2,1,0:T(8,128)(2,1)S(1)} %bitcast.359, bf16[1,2048,256]{2,1,0:T(8,128)(2,1)} %param.34), kind=kOutput, calls=%fused_computation.11 | convolution fusion | flops 672235520 | bytes 5046272 | tf_op jit(solution)/shard_map/secf,efd->secd/dot_general | solution.py:264
  102.0 1.3 convolution_bitcast_fusion.4
  103.2 3.9 %fusion.1 = bf16[8,1,40,2048]{3,2,0,1:T(8,128)(2,1)} fusion(bf16[1,256,2048]{2,1,0:T(8,128)(2,1)S(1)} %copy-done, f32[8,1,40,256]{3,2,0,1:T(8,128)} %convolution_bitcast_fusion.4, bf16[8,40,2048]{2,1,0:T(8,128)(2,1)S(1)} %bitcast.361, bf16[1,2048,256]{2,1,0:T(8,128)(2,1)} %param.34), kind=kOutput, calls=%fused_computation.10 | convolution fusion | flops 672235520 | bytes 5046272 | tf_op jit(solution)/shard_map/secf,efd->secd/dot_general | solution.py:264
  110.6 1.3 convolution_bitcast_fusion.6
  111.8 3.9 %fusion = bf16[8,1,40,2048]{3,2,0,1:T(8,128)(2,1)} fusion(bf16[1,256,2048]{2,1,0:T(8,128)(2,1)S(1)} %copy-done, f32[8,1,40,256]{3,2,0,1:T(8,128)} %convolution_bitcast_fusion.6, bf16[8,40,2048]{2,1,0:T(8,128)(2,1)S(1)} %bitcast.363, bf16[1,2048,256]{2,1,0:T(8,128)(2,1)} %param.34), kind=kOutput, calls=%fused_computation.9 | convolution fusion | flops 672235520 | bytes 5046272 | tf_op jit(solution)/shard_map/secf,efd->secd/dot_general | solution.py:264
  118.3 1.3 fusion.89
  121.7 5.0 %convolution_convert_fusion = bf16[512,2048]{1,0:T(8,128)(2,1)} fusion(bf16[128,2048]{1,0:T(8,128)(2,1)S(1)} %copy-done.34, f32[512,128]{1,0:T(8,128)S(1)} %fusion.95, bf16[512,2048]{1,0:T(8,128)(2,1)S(1)} %bitcast.353, bf16[2048,128]{1,0:T(8,128)(2,1)} %param.38), kind=kOutput, calls=%fused_computation | convolution fusion | flops 538312704 | bytes 5505024 | tf_op jit(solution)/shard_map/dot_general | solution.py:249
  126.7 1.3 slice_bitcast_fusion.7
  130.5 1.3 fusion.30
  133.6 2.0 fusion.34
  135.6 1.5 collective-permute-start.21
  138.3 1.8 fusion.38
  142.9 1.8 fusion.42
  144.7 1.5 collective-permute-start.6
  146.2 1.2 copy-done.2
  147.5 14.1 %attention.1 = bf16[256,256]{1,0:T(8,128)(2,1)S(1)} custom-call(s32[1]{0:T(128)} %bitcast.rank_ref, f32[2]{0:T(128)S(1)} %copy-done.3, bf16[256,256]{1,0:T(8,128)(2,1)S(1)} %get-tuple-element.41.queries_ref, bf16[2048,256]{1,0:T(8,128)(2,1)S(1)} %copy-done.2, f32[1,128]{1,0:T(1,128)S(1)} %bitcast.351), custom_call_target="tpu_custom_call" | custom-call | flops 1073741824 | bytes 1048576 | tf_op jit(solution)/shard_map/attention/pallas_call | solution.py:106
  164.7 1.3 fusion.37
  166.0 9.4 %collective-permute-start.22 = (bf16[40,2048]{1,0:T(8,128)(2,1)S(1)}, bf16[40,2048]{1,0:T(8,128)(2,1)S(1)}, u32[]{:S(2)}, u32[]{:S(2)}) collective-permute-start(bf16[40,2048]{1,0:T(8,128)(2,1)S(1)} %get-tuple-element.35), channel_id=1, source_target_pairs={{0,16},{4,20},{8,24},{12,28},{16,0},{20,4},{24,8},{28,12},{1,17},{... | collective-permute-start | bytes 491528 | tf_op jit(solution)/shard_map/ppermute | solution.py:125
  177.9 4.1 %collective-permute-done.7 = bf16[40,2048]{1,0:T(8,128)(2,1)S(1)} collective-permute-done((bf16[40,2048]{1,0:T(8,128)(2,1)S(1)}, bf16[40,2048]{1,0:T(8,128)(2,1)S(1)}, u32[]{:S(2)}, u32[]{:S(2)}) %collective-permute-start.7) | collective-permute-done | bytes 163872 | tf_op jit(solution)/shard_map/ppermute | solution.py:125
  182.0 5.3 %collective-permute-done.14 = bf16[40,2048]{1,0:T(8,128)(2,1)S(1)} collective-permute-done((bf16[40,2048]{1,0:T(8,128)(2,1)S(1)}, bf16[40,2048]{1,0:T(8,128)(2,1)S(1)}, u32[]{:S(2)}, u32[]{:S(2)}) %collective-permute-start.14) | collective-permute-done | bytes 163872 | tf_op jit(solution)/shard_map/ppermute | solution.py:125
  187.4 6.7 %collective-permute-done.15 = bf16[40,2048]{1,0:T(8,128)(2,1)S(1)} collective-permute-done((bf16[40,2048]{1,0:T(8,128)(2,1)S(1)}, bf16[40,2048]{1,0:T(8,128)(2,1)S(1)}, u32[]{:S(2)}, u32[]{:S(2)}) %collective-permute-start.15) | collective-permute-done | bytes 163872 | tf_op jit(solution)/shard_map/ppermute | solution.py:125
  194.1 4.9 %collective-permute-start.31 = (bf16[40,2048]{1,0:T(8,128)(2,1)S(1)}, bf16[40,2048]{1,0:T(8,128)(2,1)S(1)}, u32[]{:S(2)}, u32[]{:S(2)}) collective-permute-start(bf16[40,2048]{1,0:T(8,128)(2,1)S(1)} %get-tuple-element.32), channel_id=1, source_target_pairs={{0,28},{4,24},{8,20},{12,16},{16,12},{20,8},{24,4},{28,0},{1,29},{... | collective-permute-start | bytes 491528 | tf_op jit(solution)/shard_map/ppermute | solution.py:125
  199.1 6.2 %collective-permute-done.23 = bf16[40,2048]{1,0:T(8,128)(2,1)S(1)} collective-permute-done((bf16[40,2048]{1,0:T(8,128)(2,1)S(1)}, bf16[40,2048]{1,0:T(8,128)(2,1)S(1)}, u32[]{:S(2)}, u32[]{:S(2)}) %collective-permute-start.23) | collective-permute-done | bytes 163872 | tf_op jit(solution)/shard_map/ppermute | solution.py:125
  205.3 6.2 %collective-permute-done.31 = bf16[40,2048]{1,0:T(8,128)(2,1)S(1)} collective-permute-done((bf16[40,2048]{1,0:T(8,128)(2,1)S(1)}, bf16[40,2048]{1,0:T(8,128)(2,1)S(1)}, u32[]{:S(2)}, u32[]{:S(2)}) %collective-permute-start.31) | collective-permute-done | bytes 163872 | tf_op jit(solution)/shard_map/ppermute | solution.py:125
  214.7 6.2 %collective-permute-done.1 = bf16[1,64,2048]{2,1,0:T(8,128)(2,1)S(1)} collective-permute-done((bf16[1,64,2048]{2,1,0:T(8,128)(2,1)S(1)}, bf16[1,64,2048]{2,1,0:T(8,128)(2,1)S(1)}, u32[]{:S(2)}, u32[]{:S(2)}) %collective-permute-start.1) | collective-permute-done | bytes 262176 | tf_op jit(solution)/shard_map/ppermute | solution.py:125
  221.7 9.3 %collective-permute-done.35 = bf16[1,128,2048]{2,1,0:T(8,128)(2,1)S(1)} collective-permute-done((bf16[1,128,2048]{2,1,0:T(8,128)(2,1)S(1)}, bf16[1,128,2048]{2,1,0:T(8,128)(2,1)S(1)}, u32[]{:S(2)}, u32[]{:S(2)}) %collective-permute-start.35) | collective-permute-done | bytes 524320 | tf_op jit(solution)/shard_map/ppermute | solution.py:125
  231.0 1.3 fusion.5
  (209 shorter events, 50.9 us)
Async XLA Ops:
  7.2 78.4 %copy-start = (bf16[1,256,2048]{2,1,0:T(8,128)(2,1)S(1)}, bf16[1,256,2048]{2,1,0:T(8,128)(2,1)}, u32[]{:S(2)}) copy-start(bf16[1,256,2048]{2,1,0:T(8,128)(2,1)} %param.36) | copy-start | bytes 3145732
  7.2 139.0 %all-gather.2.cloned.1.call-start = ((), (), s32[]{:S(2)}) async-start(), calls=%async_computation | async-start | bytes 1179648 | tf_op jit(solution)/shard_map/all_gather | solution.py:195
  12.2 10.2 %copy-start.35 = (bf16[2048,64]{0,1:T(8,128)(2,1)S(1)}, bf16[2048,64]{0,1:T(8,128)(2,1)}, u32[]{:S(2)}) copy-start(bf16[2048,64]{0,1:T(8,128)(2,1)} %param.24) | copy-start | bytes 786436
  13.2 21.8 %collective-permute-start.24 = (bf16[40,2048]{1,0:T(8,128)(2,1)}, bf16[40,2048]{1,0:T(8,128)(2,1)}, u32[]{:S(2)}, u32[]{:S(2)}) collective-permute-start(bf16[40,2048]{1,0:T(8,128)(2,1)} %get-tuple-element.6), channel_id=1, source_target_pairs={{0,24},{4,28},{8,16},{12,20},{16,8},{20,12},{24,0},{28,4},{1,25},{... | collective-permute-start | bytes 491528 | tf_op jit(solution)/shard_map/ppermute | solution.py:125
  13.7 25.0 %collective-permute-start.25 = (bf16[40,2048]{1,0:T(8,128)(2,1)}, bf16[40,2048]{1,0:T(8,128)(2,1)}, u32[]{:S(2)}, u32[]{:S(2)}) collective-permute-start(bf16[40,2048]{1,0:T(8,128)(2,1)} %get-tuple-element.7), channel_id=1, source_target_pairs={{0,28},{4,24},{8,20},{12,16},{16,12},{20,8},{24,4},{28,0},{1,29},{... | collective-permute-start | bytes 491528 | tf_op jit(solution)/shard_map/ppermute | solution.py:125
  15.2 26.2 %collective-permute-start.16 = (bf16[40,2048]{1,0:T(8,128)(2,1)}, bf16[40,2048]{1,0:T(8,128)(2,1)}, u32[]{:S(2)}, u32[]{:S(2)}) collective-permute-start(bf16[40,2048]{1,0:T(8,128)(2,1)} %get-tuple-element.9), channel_id=1, source_target_pairs={{0,16},{4,20},{8,24},{12,28},{16,0},{20,4},{24,8},{28,12},{1,17},{... | collective-permute-start | bytes 491528 | tf_op jit(solution)/shard_map/ppermute | solution.py:125
  17.4 24.7 %collective-permute-start.17 = (bf16[40,2048]{1,0:T(8,128)(2,1)}, bf16[40,2048]{1,0:T(8,128)(2,1)}, u32[]{:S(2)}, u32[]{:S(2)}) collective-permute-start(bf16[40,2048]{1,0:T(8,128)(2,1)} %get-tuple-element.8), channel_id=1, source_target_pairs={{0,20},{4,16},{8,28},{12,24},{16,4},{20,0},{24,12},{28,8},{1,21},{... | collective-permute-start | bytes 491528 | tf_op jit(solution)/shard_map/ppermute | solution.py:125
  19.1 6.4 %copy-start.32 = (bf16[2048,128]{1,0:T(8,128)(2,1)S(1)}, bf16[2048,128]{1,0:T(8,128)(2,1)}, u32[]{:S(2)}) copy-start(bf16[2048,128]{1,0:T(8,128)(2,1)} %param.22) | copy-start | bytes 1572868
  19.1 25.4 %collective-permute-start.8 = (bf16[40,2048]{1,0:T(8,128)(2,1)}, bf16[40,2048]{1,0:T(8,128)(2,1)}, u32[]{:S(2)}, u32[]{:S(2)}) collective-permute-start(bf16[40,2048]{1,0:T(8,128)(2,1)} %get-tuple-element.11), channel_id=1, source_target_pairs={{0,8},{4,12},{8,0},{12,4},{16,24},{20,28},{24,16},{28,20},{1,9},{5... | collective-permute-start | bytes 491528 | tf_op jit(solution)/shard_map/ppermute | solution.py:125
  34.1 47.1 %copy-start.14 = (bf16[1,128,2048]{2,1,0:T(8,128)(2,1)}, bf16[1,128,2048]{2,1,0:T(8,128)(2,1)S(1)}, u32[]{:S(2)}) copy-start(bf16[1,128,2048]{2,1,0:T(8,128)(2,1)S(1)} %fusion.73) | copy-start | bytes 1572868
  35.0 11.1 %collective-permute-start.9 = (bf16[40,2048]{1,0:T(8,128)(2,1)S(1)}, bf16[40,2048]{1,0:T(8,128)(2,1)S(1)}, u32[]{:S(2)}, u32[]{:S(2)}) collective-permute-start(bf16[40,2048]{1,0:T(8,128)(2,1)S(1)} %copy-done.37), channel_id=1, source_target_pairs={{0,12},{4,8},{8,4},{12,0},{16,28},{20,24},{24,20},{28,16},{1,13},{... | collective-permute-start | bytes 491528 | tf_op jit(solution)/shard_map/ppermute | solution.py:125
  38.7 9.0 %collective-permute-start.2 = (bf16[40,2048]{1,0:T(8,128)(2,1)S(1)}, bf16[40,2048]{1,0:T(8,128)(2,1)S(1)}, u32[]{:S(2)}, u32[]{:S(2)}) collective-permute-start(bf16[40,2048]{1,0:T(8,128)(2,1)S(1)} %copy-done.36), channel_id=1, source_target_pairs={{0,4},{4,0},{8,12},{12,8},{16,20},{20,16},{24,28},{28,24},{1,5},{5... | collective-permute-start | bytes 491528 | tf_op jit(solution)/shard_map/ppermute | solution.py:125
  41.4 39.8 %collective-permute-start.32 = (bf16[1,128,2048]{2,1,0:T(8,128)(2,1)S(1)}, bf16[1,128,2048]{2,1,0:T(8,128)(2,1)S(1)}, u32[]{:S(2)}, u32[]{:S(2)}) collective-permute-start(bf16[1,128,2048]{2,1,0:T(8,128)(2,1)S(1)} %fusion.73), channel_id=1, source_target_pairs={{0,2},{1,3},{2,0},{3,1},{4,6},{5,7},{6,4},{7,5},{8,10},{9,11},{10,... | collective-permute-start | bytes 1572872 | tf_op jit(solution)/shard_map/ppermute | solution.py:125
  42.1 21.2 %collective-permute-start.26 = (bf16[1,2,40,2048]{3,2,1,0:T(8,128)(2,1)S(1)}, bf16[1,2,40,2048]{3,2,1,0:T(8,128)(2,1)S(1)}, u32[]{:S(2)}, u32[]{:S(2)}) collective-permute-start(bf16[1,2,40,2048]{3,2,1,0:T(8,128)(2,1)S(1)} %maximum_bitcast_fusion.3), channel_id=1, source_target_pairs={{0,2},{1,3},{2,0},{3,1},{4,6},{5,7},{6,4},{7,5},{8,10},{9,11},{10,... | collective-permute-start | bytes 983048 | tf_op jit(solution)/shard_map/ppermute | solution.py:125
  44.5 25.8 %copy-start.20 = (bf16[1,2,40,2048]{3,2,1,0:T(8,128)(2,1)}, bf16[1,2,40,2048]{3,2,1,0:T(8,128)(2,1)S(1)}, u32[]{:S(2)}) copy-start(bf16[1,2,40,2048]{3,2,1,0:T(8,128)(2,1)S(1)} %maximum_bitcast_fusion.2) | copy-start | bytes 983044
  44.5 25.8 %collective-permute-start.18 = (bf16[1,2,40,2048]{3,2,1,0:T(8,128)(2,1)S(1)}, bf16[1,2,40,2048]{3,2,1,0:T(8,128)(2,1)S(1)}, u32[]{:S(2)}, u32[]{:S(2)}) collective-permute-start(bf16[1,2,40,2048]{3,2,1,0:T(8,128)(2,1)S(1)} %maximum_bitcast_fusion.2), channel_id=1, source_target_pairs={{0,2},{1,3},{2,0},{3,1},{4,6},{5,7},{6,4},{7,5},{8,10},{9,11},{10,... | collective-permute-start | bytes 983048 | tf_op jit(solution)/shard_map/ppermute | solution.py:125
  47.0 29.7 %copy-start.18 = (bf16[1,2,40,2048]{3,2,1,0:T(8,128)(2,1)}, bf16[1,2,40,2048]{3,2,1,0:T(8,128)(2,1)S(1)}, u32[]{:S(2)}) copy-start(bf16[1,2,40,2048]{3,2,1,0:T(8,128)(2,1)S(1)} %maximum_bitcast_fusion.1) | copy-start | bytes 983044
  47.0 29.7 %collective-permute-start.10 = (bf16[1,2,40,2048]{3,2,1,0:T(8,128)(2,1)S(1)}, bf16[1,2,40,2048]{3,2,1,0:T(8,128)(2,1)S(1)}, u32[]{:S(2)}, u32[]{:S(2)}) collective-permute-start(bf16[1,2,40,2048]{3,2,1,0:T(8,128)(2,1)S(1)} %maximum_bitcast_fusion.1), channel_id=1, source_target_pairs={{0,2},{1,3},{2,0},{3,1},{4,6},{5,7},{6,4},{7,5},{8,10},{9,11},{10,... | collective-permute-start | bytes 983048 | tf_op jit(solution)/shard_map/ppermute | solution.py:125
  47.7 32.5 %copy-start.16 = (bf16[1,2,40,2048]{3,2,1,0:T(8,128)(2,1)}, bf16[1,2,40,2048]{3,2,1,0:T(8,128)(2,1)S(1)}, u32[]{:S(2)}) copy-start(bf16[1,2,40,2048]{3,2,1,0:T(8,128)(2,1)S(1)} %maximum_bitcast_fusion) | copy-start | bytes 983044
  47.7 32.5 %collective-permute-start.3 = (bf16[1,2,40,2048]{3,2,1,0:T(8,128)(2,1)S(1)}, bf16[1,2,40,2048]{3,2,1,0:T(8,128)(2,1)S(1)}, u32[]{:S(2)}, u32[]{:S(2)}) collective-permute-start(bf16[1,2,40,2048]{3,2,1,0:T(8,128)(2,1)S(1)} %maximum_bitcast_fusion), channel_id=1, source_target_pairs={{0,2},{1,3},{2,0},{3,1},{4,6},{5,7},{6,4},{7,5},{8,10},{9,11},{10,... | collective-permute-start | bytes 983048 | tf_op jit(solution)/shard_map/ppermute | solution.py:125
  63.3 19.6 %collective-permute-start.27 = (bf16[2,2,40,2048]{3,2,1,0:T(8,128)(2,1)S(1)}, bf16[2,2,40,2048]{3,2,1,0:T(8,128)(2,1)S(1)}, u32[]{:S(2)}, u32[]{:S(2)}) collective-permute-start(bf16[2,2,40,2048]{3,2,1,0:T(8,128)(2,1)S(1)} %pad_maximum_fusion.13), channel_id=1, source_target_pairs={{0,1},{1,0},{2,3},{3,2},{4,5},{5,4},{6,7},{7,6},{8,9},{9,8},{10,11... | collective-permute-start | bytes 1966088 | tf_op jit(solution)/shard_map/ppermute | solution.py:125
  70.3 7.4 %copy-start.29 = (bf16[1,2,40,2048]{3,2,1,0:T(8,128)(2,1)}, bf16[1,2,40,2048]{3,2,1,0:T(8,128)(2,1)S(1)}, u32[]{:S(2)}) copy-start(bf16[1,2,40,2048]{3,2,1,0:T(8,128)(2,1)S(1)} %collective-permute-done.18) | copy-start | bytes 983044
  71.2 20.3 %collective-permute-start.19 = (bf16[2,2,40,2048]{3,2,1,0:T(8,128)(2,1)}, bf16[2,2,40,2048]{3,2,1,0:T(8,128)(2,1)}, u32[]{:S(2)}, u32[]{:S(2)}) collective-permute-start(bf16[2,2,40,2048]{3,2,1,0:T(8,128)(2,1)} %pad_maximum_fusion.11), channel_id=1, source_target_pairs={{0,1},{1,0},{2,3},{3,2},{4,5},{5,4},{6,7},{7,6},{8,9},{9,8},{10,11... | collective-permute-start | bytes 1966088 | tf_op jit(solution)/shard_map/ppermute | solution.py:125
  77.7 23.0 %collective-permute-start.11 = (bf16[2,2,40,2048]{3,2,1,0:T(8,128)(2,1)}, bf16[2,2,40,2048]{3,2,1,0:T(8,128)(2,1)}, u32[]{:S(2)}, u32[]{:S(2)}) collective-permute-start(bf16[2,2,40,2048]{3,2,1,0:T(8,128)(2,1)} %pad_maximum_fusion.9), channel_id=1, source_target_pairs={{0,1},{1,0},{2,3},{3,2},{4,5},{5,4},{6,7},{7,6},{8,9},{9,8},{10,11... | collective-permute-start | bytes 1966088 | tf_op jit(solution)/shard_map/ppermute | solution.py:125
  81.2 28.0 %collective-permute-start.4 = (bf16[2,2,40,2048]{3,2,1,0:T(8,128)(2,1)}, bf16[2,2,40,2048]{3,2,1,0:T(8,128)(2,1)}, u32[]{:S(2)}, u32[]{:S(2)}) collective-permute-start(bf16[2,2,40,2048]{3,2,1,0:T(8,128)(2,1)} %pad_maximum_fusion.7), channel_id=1, source_target_pairs={{0,1},{1,0},{2,3},{3,2},{4,5},{5,4},{6,7},{7,6},{8,9},{9,8},{10,11... | collective-permute-start | bytes 1966088 | tf_op jit(solution)/shard_map/ppermute | solution.py:125
  82.5 35.8 %collective-permute-start.33 = (bf16[2,128,2048]{2,1,0:T(8,128)(2,1)}, bf16[2,128,2048]{2,1,0:T(8,128)(2,1)}, u32[]{:S(2)}, u32[]{:S(2)}) collective-permute-start(bf16[2,128,2048]{2,1,0:T(8,128)(2,1)} %pad_maximum_fusion.5), channel_id=1, source_target_pairs={{0,1},{1,0},{2,3},{3,2},{4,5},{5,4},{6,7},{7,6},{8,9},{9,8},{10,11... | collective-permute-start | bytes 3145736 | tf_op jit(solution)/shard_map/ppermute | solution.py:125
  91.5 37.7 %collective-permute-start.28 = (bf16[2,2,40,2048]{3,2,1,0:T(8,128)(2,1)}, bf16[2,2,40,2048]{3,2,1,0:T(8,128)(2,1)}, u32[]{:S(2)}, u32[]{:S(2)}) collective-permute-start(bf16[2,2,40,2048]{3,2,1,0:T(8,128)(2,1)} %pad_maximum_fusion.14), channel_id=1, source_target_pairs={{0,1},{1,0},{2,3},{3,2},{4,5},{5,4},{6,7},{7,6},{8,9},{9,8},{10,11... | collective-permute-start | bytes 1966088 | tf_op jit(solution)/shard_map/ppermute | solution.py:125
  100.2 32.1 %collective-permute-start.20 = (bf16[2,2,40,2048]{3,2,1,0:T(8,128)(2,1)}, bf16[2,2,40,2048]{3,2,1,0:T(8,128)(2,1)}, u32[]{:S(2)}, u32[]{:S(2)}) collective-permute-start(bf16[2,2,40,2048]{3,2,1,0:T(8,128)(2,1)} %pad_maximum_fusion.12), channel_id=1, source_target_pairs={{0,1},{1,0},{2,3},{3,2},{4,5},{5,4},{6,7},{7,6},{8,9},{9,8},{10,11... | collective-permute-start | bytes 1966088 | tf_op jit(solution)/shard_map/ppermute | solution.py:125
  109.2 27.9 %collective-permute-start.12 = (bf16[2,2,40,2048]{3,2,1,0:T(8,128)(2,1)}, bf16[2,2,40,2048]{3,2,1,0:T(8,128)(2,1)}, u32[]{:S(2)}, u32[]{:S(2)}) collective-permute-start(bf16[2,2,40,2048]{3,2,1,0:T(8,128)(2,1)} %pad_maximum_fusion.10), channel_id=1, source_target_pairs={{0,1},{1,0},{2,3},{3,2},{4,5},{5,4},{6,7},{7,6},{8,9},{9,8},{10,11... | collective-permute-start | bytes 1966088 | tf_op jit(solution)/shard_map/ppermute | solution.py:125
  117.8 22.8 %collective-permute-start.5 = (bf16[2,2,40,2048]{3,2,1,0:T(8,128)(2,1)}, bf16[2,2,40,2048]{3,2,1,0:T(8,128)(2,1)}, u32[]{:S(2)}, u32[]{:S(2)}) collective-permute-start(bf16[2,2,40,2048]{3,2,1,0:T(8,128)(2,1)} %pad_maximum_fusion.8), channel_id=1, source_target_pairs={{0,1},{1,0},{2,3},{3,2},{4,5},{5,4},{6,7},{7,6},{8,9},{9,8},{10,11... | collective-permute-start | bytes 1966088 | tf_op jit(solution)/shard_map/ppermute | solution.py:125
  129.0 83.2 %collective-permute-start.34 = (bf16[2,128,2048]{2,1,0:T(8,128)(2,1)}, bf16[2,128,2048]{2,1,0:T(8,128)(2,1)S(1)}, u32[]{:S(2)}, u32[]{:S(2)}) collective-permute-start(bf16[2,128,2048]{2,1,0:T(8,128)(2,1)} %pad_maximum_fusion.6), channel_id=1, source_target_pairs={{0,1},{1,0},{2,3},{3,2},{4,5},{5,4},{6,7},{7,6},{8,9},{9,8},{10,11... | collective-permute-start | bytes 3145736 | tf_op jit(solution)/shard_map/ppermute | solution.py:125
  131.7 30.4 %collective-permute-start.29 = (bf16[1,2,40,2048]{3,2,1,0:T(8,128)(2,1)S(1)}, bf16[1,2,40,2048]{3,2,1,0:T(8,128)(2,1)}, u32[]{:S(2)}, u32[]{:S(2)}) collective-permute-start(bf16[1,2,40,2048]{3,2,1,0:T(8,128)(2,1)S(1)} %fusion.30), channel_id=1, source_target_pairs={{0,2},{1,3},{2,0},{3,1},{4,6},{5,7},{6,4},{7,5},{8,10},{9,11},{10,... | collective-permute-start | bytes 983048 | tf_op jit(solution)/shard_map/ppermute | solution.py:125
  135.6 29.0 %collective-permute-start.21 = (bf16[1,2,40,2048]{3,2,1,0:T(8,128)(2,1)}, bf16[1,2,40,2048]{3,2,1,0:T(8,128)(2,1)}, u32[]{:S(2)}, u32[]{:S(2)}) collective-permute-start(bf16[1,2,40,2048]{3,2,1,0:T(8,128)(2,1)} %fusion.34), channel_id=1, source_target_pairs={{0,2},{1,3},{2,0},{3,1},{4,6},{5,7},{6,4},{7,5},{8,10},{9,11},{10,... | collective-permute-start | bytes 983048 | tf_op jit(solution)/shard_map/ppermute | solution.py:125
  140.1 36.5 %collective-permute-start.13 = (bf16[1,2,40,2048]{3,2,1,0:T(8,128)(2,1)}, bf16[1,2,40,2048]{3,2,1,0:T(8,128)(2,1)}, u32[]{:S(2)}, u32[]{:S(2)}) collective-permute-start(bf16[1,2,40,2048]{3,2,1,0:T(8,128)(2,1)} %fusion.38), channel_id=1, source_target_pairs={{0,2},{1,3},{2,0},{3,1},{4,6},{5,7},{6,4},{7,5},{8,10},{9,11},{10,... | collective-permute-start | bytes 983048 | tf_op jit(solution)/shard_map/ppermute | solution.py:125
  144.7 21.3 %collective-permute-start.6 = (bf16[1,2,40,2048]{3,2,1,0:T(8,128)(2,1)}, bf16[1,2,40,2048]{3,2,1,0:T(8,128)(2,1)}, u32[]{:S(2)}, u32[]{:S(2)}) collective-permute-start(bf16[1,2,40,2048]{3,2,1,0:T(8,128)(2,1)} %fusion.42), channel_id=1, source_target_pairs={{0,2},{1,3},{2,0},{3,1},{4,6},{5,7},{6,4},{7,5},{8,10},{9,11},{10,... | collective-permute-start | bytes 983048 | tf_op jit(solution)/shard_map/ppermute | solution.py:125
  147.5 14.1 %copy-start.31 = (bf16[256,2048]{1,0:T(8,128)(2,1)S(1)}, bf16[256,2048]{1,0:T(8,128)(2,1)}, u32[]{:S(2)}) copy-start(bf16[256,2048]{1,0:T(8,128)(2,1)} %param.29) | copy-start | bytes 3145732
  162.2 49.3 %collective-permute-start = (bf16[2,64,2048]{2,1,0:T(8,128)(2,1)S(1)}, bf16[2,64,2048]{2,1,0:T(8,128)(2,1)S(1)}, u32[]{:S(2)}, u32[]{:S(2)}) collective-permute-start(bf16[2,64,2048]{2,1,0:T(8,128)(2,1)S(1)} %pad_maximum_fusion.15), channel_id=1, source_target_pairs={{0,1},{1,0},{2,3},{3,2},{4,5},{5,4},{6,7},{7,6},{8,9},{9,8},{10,11... | collective-permute-start | bytes 1572872 | tf_op jit(solution)/shard_map/ppermute | solution.py:125
  164.6 10.8 %copy-start.12 = (f32[2,2,40,2048]{3,2,1,0:T(8,128)S(1)}, f32[2,2,40,2048]{3,2,1,0:T(8,128)}, u32[]{:S(2)}) copy-start(f32[2,2,40,2048]{3,2,1,0:T(8,128)} %copy-done.11) | copy-start | bytes 3932164
  164.6 40.7 %collective-permute-start.30 = (bf16[40,2048]{1,0:T(8,128)(2,1)S(1)}, bf16[40,2048]{1,0:T(8,128)(2,1)S(1)}, u32[]{:S(2)}, u32[]{:S(2)}) collective-permute-start(bf16[40,2048]{1,0:T(8,128)(2,1)S(1)} %get-tuple-element.33), channel_id=1, source_target_pairs={{0,24},{4,28},{8,16},{12,20},{16,8},{20,12},{24,0},{28,4},{1,25},{... | collective-permute-start | bytes 491528 | tf_op jit(solution)/shard_map/ppermute | solution.py:125
  166.0 28.1 %collective-permute-start.22 = (bf16[40,2048]{1,0:T(8,128)(2,1)S(1)}, bf16[40,2048]{1,0:T(8,128)(2,1)S(1)}, u32[]{:S(2)}, u32[]{:S(2)}) collective-permute-start(bf16[40,2048]{1,0:T(8,128)(2,1)S(1)} %get-tuple-element.35), channel_id=1, source_target_pairs={{0,16},{4,20},{8,24},{12,28},{16,0},{20,4},{24,8},{28,12},{1,17},{... | collective-permute-start | bytes 491528 | tf_op jit(solution)/shard_map/ppermute | solution.py:125
  176.6 5.4 %collective-permute-start.7 = (bf16[40,2048]{1,0:T(8,128)(2,1)S(1)}, bf16[40,2048]{1,0:T(8,128)(2,1)S(1)}, u32[]{:S(2)}, u32[]{:S(2)}) collective-permute-start(bf16[40,2048]{1,0:T(8,128)(2,1)S(1)} %get-tuple-element.38), channel_id=1, source_target_pairs={{0,4},{4,0},{8,12},{12,8},{16,20},{20,16},{24,28},{28,24},{1,5},{5... | collective-permute-start | bytes 491528 | tf_op jit(solution)/shard_map/ppermute | solution.py:125
  182.0 5.3 %collective-permute-start.14 = (bf16[40,2048]{1,0:T(8,128)(2,1)S(1)}, bf16[40,2048]{1,0:T(8,128)(2,1)S(1)}, u32[]{:S(2)}, u32[]{:S(2)}) collective-permute-start(bf16[40,2048]{1,0:T(8,128)(2,1)S(1)} %get-tuple-element.37), channel_id=1, source_target_pairs={{0,8},{4,12},{8,0},{12,4},{16,24},{20,28},{24,16},{28,20},{1,9},{5... | collective-permute-start | bytes 491528 | tf_op jit(solution)/shard_map/ppermute | solution.py:125
  187.3 6.8 %collective-permute-start.15 = (bf16[40,2048]{1,0:T(8,128)(2,1)S(1)}, bf16[40,2048]{1,0:T(8,128)(2,1)S(1)}, u32[]{:S(2)}, u32[]{:S(2)}) collective-permute-start(bf16[40,2048]{1,0:T(8,128)(2,1)S(1)} %get-tuple-element.36), channel_id=1, source_target_pairs={{0,12},{4,8},{8,4},{12,0},{16,28},{20,24},{24,20},{28,16},{1,13},{... | collective-permute-start | bytes 491528 | tf_op jit(solution)/shard_map/ppermute | solution.py:125
  194.1 11.1 %collective-permute-start.23 = (bf16[40,2048]{1,0:T(8,128)(2,1)S(1)}, bf16[40,2048]{1,0:T(8,128)(2,1)S(1)}, u32[]{:S(2)}, u32[]{:S(2)}) collective-permute-start(bf16[40,2048]{1,0:T(8,128)(2,1)S(1)} %get-tuple-element.34), channel_id=1, source_target_pairs={{0,20},{4,16},{8,28},{12,24},{16,4},{20,0},{24,12},{28,8},{1,21},{... | collective-permute-start | bytes 491528 | tf_op jit(solution)/shard_map/ppermute | solution.py:125
  194.1 17.3 %collective-permute-start.31 = (bf16[40,2048]{1,0:T(8,128)(2,1)S(1)}, bf16[40,2048]{1,0:T(8,128)(2,1)S(1)}, u32[]{:S(2)}, u32[]{:S(2)}) collective-permute-start(bf16[40,2048]{1,0:T(8,128)(2,1)S(1)} %get-tuple-element.32), channel_id=1, source_target_pairs={{0,28},{4,24},{8,20},{12,16},{16,12},{20,8},{24,4},{28,0},{1,29},{... | collective-permute-start | bytes 491528 | tf_op jit(solution)/shard_map/ppermute | solution.py:125
  211.7 9.2 %collective-permute-start.1 = (bf16[1,64,2048]{2,1,0:T(8,128)(2,1)S(1)}, bf16[1,64,2048]{2,1,0:T(8,128)(2,1)S(1)}, u32[]{:S(2)}, u32[]{:S(2)}) collective-permute-start(bf16[1,64,2048]{2,1,0:T(8,128)(2,1)S(1)} %fusion.46), channel_id=1, source_target_pairs={{0,2},{1,3},{2,0},{3,1},{4,6},{5,7},{6,4},{7,5},{8,10},{9,11},{10,... | collective-permute-start | bytes 786440 | tf_op jit(solution)/shard_map/ppermute | solution.py:125
  213.4 17.7 %collective-permute-start.35 = (bf16[1,128,2048]{2,1,0:T(8,128)(2,1)S(1)}, bf16[1,128,2048]{2,1,0:T(8,128)(2,1)S(1)}, u32[]{:S(2)}, u32[]{:S(2)}) collective-permute-start(bf16[1,128,2048]{2,1,0:T(8,128)(2,1)S(1)} %fusion.13), channel_id=1, source_target_pairs={{0,2},{1,3},{2,0},{3,1},{4,6},{5,7},{6,4},{7,5},{8,10},{9,11},{10,... | collective-permute-start | bytes 1572872 | tf_op jit(solution)/shard_map/ppermute | solution.py:125
  220.9 11.4 %copy-start.1 = (bf16[1,256,2048]{2,1,0:T(8,128)(2,1)S(1)}, bf16[1,256,2048]{2,1,0:T(8,128)(2,1)}, u32[]{:S(2)}) copy-start(bf16[1,256,2048]{2,1,0:T(8,128)(2,1)} %param.36) | copy-start | bytes 3145732
  (30 other events, 75.5 us)
Sparse Core Ops, SparseCore 0:
  34.1 39.6 all-gather.1

commit v2 on v1

--- a/solution.py
+++ b/solution.py
@@ -13,7 +13,6 @@
 
 EPS = 1e-06
 NEG = -1e30
-GROUPS = 4
 
 
 def normalize(activations, scaling):
@@ -129,27 +128,27 @@
     places = {0: block}
     distance = size // 2
     while distance:
-        held = sorted(places)
-        moved = swap(jnp.stack([places[p] for p in held]), axis, size, distance)
-        places.update({p ^ distance: moved[i] for i, p in enumerate(held)})
+        for place in sorted(places):
+            places[place ^ distance] = swap(places[place], axis, size, distance)
         distance //= 2
-    return jnp.stack([places[p] for p in range(size)])
+    return [places[place] for place in range(size)]
 
 
 def scatter_near(partials, axis, size):
-    sums = {p: partials[p] for p in range(size)}
+    sums = dict(enumerate(partials))
     distance = 1
     while distance < size:
-        kept = [p for p in sorted(sums) if not p & distance]
-        sent = jnp.stack([sums[p ^ distance].astype(jnp.bfloat16) for p in kept])
-        moved = swap(sent, axis, size, distance).astype(jnp.float32)
-        sums = {p: sums[p].astype(jnp.float32) + moved[i] for i, p in enumerate(kept)}
+        kept = [place for place in sorted(sums) if not place & distance]
+        moved = {
+            place: swap(sums[place ^ distance].astype(jnp.bfloat16), axis, size, distance)
+            for place in kept
+        }
+        sums = {
+            place: sums[place].astype(jnp.float32) + moved[place].astype(jnp.float32)
+            for place in kept
+        }
         distance *= 2
     return sums[0]
-
-
-def exchange(blocks, axis, size):
-    return [blocks[d] if d == 0 else swap(blocks[d], axis, size, d) for d in range(size)]
 
 
 def body(
@@ -186,29 +185,33 @@
     local_heads = query_cols // HEAD
     group_size = local_heads // local_kv
     normed = normalize(mixer_input, mixer_gain)
-    joined_weight = jnp.concatenate([query_one, query_two, key_one, key_two, value_weight], axis=1)
-    projected = jnp.dot(normed, joined_weight, preferred_element_type=jnp.float32).astype(
-        jnp.bfloat16
-    )
-    query_part = projected[:, : 2 * query_cols]
-    key_values = projected[:, 2 * query_cols :]
+
+    def project(weights):
+        return jnp.concatenate(
+            [
+                jnp.dot(normed, weight, preferred_element_type=jnp.float32).astype(jnp.bfloat16)
+                for weight in weights
+            ],
+            axis=1,
+        )
+
+    key_values = project([key_one, key_two, value_weight])
+    query_part = project([query_one, query_two])
     arrived = lax.all_gather(key_values, "ep", axis=0, tiled=True)
     head_rows = attention(
         query_part, arrived, ep_rank, lambdas, head_gain, local_kv, group_size
     )
-    mixer_partial = jnp.dot(head_rows, output_weight, preferred_element_type=jnp.float32).astype(
-        jnp.bfloat16
-    )
     tp_rank = lax.axis_index("tp")
     own_rows = mixer_rows // tp_size
-    mixer_blocks = mixer_partial.reshape(tp_size, own_rows, model_width)
+
+    def mixer_place(place):
+        rows = lax.dynamic_slice_in_dim(head_rows, (tp_rank ^ place) * own_rows, own_rows, 0)
+        return jnp.dot(rows, output_weight, preferred_element_type=jnp.float32).astype(
+            jnp.bfloat16
+        )
+
     mixer_sum = scatter_near(
-        [
-            lax.dynamic_index_in_dim(mixer_blocks, tp_rank ^ place, 0, keepdims=False)
-            for place in range(tp_size)
-        ],
-        "tp",
-        tp_size,
+        [mixer_place(place) for place in range(tp_size)], "tp", tp_size
     ).astype(jnp.bfloat16)
 
     token_rows = expert_input.shape[0]
@@ -218,12 +221,7 @@
     top_count = routes.shape[1]
     capacity = max(2, 5 * token_rows * top_count // (4 * expert_count))
     slot_count = expert_count * capacity
-    direct = ep_size <= 16
     flat_routes = routes.reshape(-1)
-    if direct:
-        flat_routes = ((flat_routes // experts_local) ^ ep_rank) * experts_local + (
-            flat_routes % experts_local
-        )
     onehot = (flat_routes[:, None] == jnp.arange(expert_count, dtype=jnp.int32)[None, :]).astype(
         jnp.int32
     )
@@ -236,45 +234,47 @@
     )
     pair_rows = experts_local * capacity
     outgoing = outgoing.reshape(ep_size, pair_rows, model_width)
-    if direct:
-        received = exchange(outgoing, "ep", ep_size)
-    else:
-        received = list(lax.all_to_all(outgoing, "ep", split_axis=0, concat_axis=0, tiled=True))
-    bundle = max(1, ep_size // GROUPS)
-    expert_rows = gather_near(normed_experts, "tp", tp_size).reshape(-1, model_width)
-    shared_gated = jnp.dot(expert_rows, shared_gate, preferred_element_type=jnp.float32)
-    shared_lifted = jnp.dot(expert_rows, shared_up, preferred_element_type=jnp.float32)
-    shared_hidden = (jax.nn.silu(shared_gated) * shared_lifted).astype(jnp.bfloat16)
-    shared_part = (
-        jnp.dot(shared_hidden, shared_down, preferred_element_type=jnp.float32)
-        .astype(jnp.bfloat16)
-        .reshape(tp_size, token_rows, model_width)
-    )
-    shared_result = scatter_near(shared_part, "tp", tp_size)
-    results = []
-    for begin in range(0, ep_size, bundle):
-        held = jnp.stack(received[begin : begin + bundle])
-        slot_rows = gather_near(held, "tp", tp_size).reshape(
-            tp_size * bundle, experts_local, capacity, model_width
+    received = lax.all_to_all(outgoing, "ep", split_axis=0, concat_axis=0, tiled=True)
+    received = received.reshape(ep_size, experts_local, capacity, model_width)
+    if experts_local == 1:
+        received = received.reshape(ep_size * capacity, model_width)
+
+    def shared_expert(rows):
+        gated = jnp.dot(rows, shared_gate, preferred_element_type=jnp.float32)
+        lifted = jnp.dot(rows, shared_up, preferred_element_type=jnp.float32)
+        hidden = (jax.nn.silu(gated) * lifted).astype(jnp.bfloat16)
+        return jnp.dot(hidden, shared_down, preferred_element_type=jnp.float32).astype(
+            jnp.bfloat16
         )
-        gated = jnp.einsum("secd,edf->secf", slot_rows, expert_gate, preferred_element_type=jnp.float32)
-        lifted = jnp.einsum("secd,edf->secf", slot_rows, expert_up, preferred_element_type=jnp.float32)
-        routed_hidden = (jax.nn.silu(gated) * lifted).astype(jnp.bfloat16)
-        routed_part = (
-            jnp.einsum(
-                "secf,efd->secd", routed_hidden, expert_down, preferred_element_type=jnp.float32
+
+    def routed_expert(rows):
+        if experts_local == 1:
+            gated = jnp.dot(rows, expert_gate[0], preferred_element_type=jnp.float32)
+            lifted = jnp.dot(rows, expert_up[0], preferred_element_type=jnp.float32)
+            hidden = (jax.nn.silu(gated) * lifted).astype(jnp.bfloat16)
+            return jnp.dot(hidden, expert_down[0], preferred_element_type=jnp.float32).astype(
+                jnp.bfloat16
             )
-            .astype(jnp.bfloat16)
-            .reshape(tp_size, bundle, pair_rows, model_width)
-        )
-        total = scatter_near(routed_part, "tp", tp_size).astype(jnp.bfloat16)
-        results.extend(total[i] for i in range(bundle))
-    if direct:
-        returned = jnp.stack(exchange(results, "ep", ep_size))
-    else:
-        returned = lax.all_to_all(
-            jnp.stack(results), "ep", split_axis=0, concat_axis=0, tiled=True
-        )
+        gated = jnp.einsum("secd,edf->secf", rows, expert_gate, preferred_element_type=jnp.float32)
+        lifted = jnp.einsum("secd,edf->secf", rows, expert_up, preferred_element_type=jnp.float32)
+        hidden = (jax.nn.silu(gated) * lifted).astype(jnp.bfloat16)
+        return jnp.einsum(
+            "secf,efd->secd", hidden, expert_down, preferred_element_type=jnp.float32
+        ).astype(jnp.bfloat16)
+
+    shared_places = gather_near(normed_experts, "tp", tp_size)
+    routed_places = gather_near(received, "tp", tp_size)
+    shared_result = scatter_near([shared_expert(rows) for rows in shared_places], "tp", tp_size)
+    routed_result = scatter_near(
+        [routed_expert(rows) for rows in routed_places], "tp", tp_size
+    ).astype(jnp.bfloat16)
+    returned = lax.all_to_all(
+        routed_result.reshape(ep_size, pair_rows, model_width),
+        "ep",
+        split_axis=0,
+        concat_axis=0,
+        tiled=True,
+    )
     returned = returned.reshape(slot_count, model_width)
     spread = jnp.sum(
         jnp.where(

time: 241 us -> 215 us (0.89)
  the two profiles are of different devices: /device:TPU:22 before, /device:TPU:30 now
where the time goes in v2:
time: 215 us; the launch traced here: 214 us
  waiting for transfers between devices  63.6 us (30%)
  matrix products  55.7 us (26%)
  blocking collectives  35 us (16%)
  Pallas kernels  18.5 us (9%)
  between operations  14.4 us (7%)
  starting transfers between devices  13.1 us (6%)
  other arithmetic  10.3 us (5%)
  local copies, waits for them, and re-layouts  3.14 us (1%)
    ppermute x15, waiting for transfers between devices, swap(): return lax.ppermute(rows, axis, [(i, i ^ distance) for i in range(size)])  63.6 us
    all_to_all x1, blocking collectives, body(): lax.all_to_all(outgoing, 'ep', split_axis=0, concat_axis=0, tiled=True)  35 us
    pallas_call x1, Pallas kernels, attention(): pl.pallas_call(functools.partial(attention_kernel, (rows, chunk, local_kv...  18.5 us
    dot_general x4, matrix products, routed_expert(): jnp.dot(hidden, expert_down[0], preferred_element_type=jnp.float32)  18.2 us
    dot_general x4, matrix products, shared_expert(): jnp.dot(hidden, shared_down, preferred_element_type=jnp.float32)  8.85 us
    dot_general x3, matrix products, routed_expert(): lifted = jnp.dot(rows, expert_up[0], preferred_element_type=jnp.float32)  8.24 us
    all_to_all x1, starting transfers between devices, body(): lax.all_to_all(routed_result.reshape(ep_size, pair_rows, model_width), 'e...  6.56 us
    ppermute x15, starting transfers between devices, swap(): return lax.ppermute(rows, axis, [(i, i ^ distance) for i in range(size)])  6.5 us
  transfers between devices with their start and end apart: 17, of which 3 were waited for; matrix products, arithmetic and copies ran while one was open for 28% of the time, Pallas kernels for 9%

profile of v2, /device:TPU:30, one launch (start us, length us, event | category | flops | bytes accessed | tf_op | source)
XLA Modules:
  0.0 213.8 jit_solution(4447584078381696028)
XLA Ops:
  7.2 0.9 copy.56
  8.4 0.6 reduce-window.6
  9.6 0.7 multiply_add_fusion
  10.3 1.2 fusion.13
  11.6 0.9 fusion.15
  12.5 0.5 convolution_convert_fusion
  13.0 35.0 %all_to_all.10 = bf16[8,40,2048]{2,1,0:T(8,128)(2,1)} all-to-all(bf16[8,40,2048]{2,1,0:T(8,128)(2,1)S(1)} %bitcast.98), channel_id=1, replica_groups=mesh['ep'=8,'tp'=4] {'ep'}, dimensions={0} | all-to-all | bytes 2621440 | tf_op jit(solution)/shard_map/all_to_all | solution.py:237
  48.0 0.5 collective-permute-start.5
  48.5 1.5 collective-permute-start.11
  50.4 0.5 convolution_convert_fusion.17
  50.9 29.1 %collective-permute-done.5 = bf16[320,2048]{1,0:T(8,128)(2,1)} collective-permute-done((bf16[320,2048]{1,0:T(8,128)(2,1)}, bf16[320,2048]{1,0:T(8,128)(2,1)}, u32[]{:S(2)}, u32[]{:S(2)}) %collective-permute-start.5) | collective-permute-done | bytes 1310752 | tf_op jit(solution)/shard_map/ppermute | solution.py:124
  80.0 0.5 convolution_convert_fusion.16
  80.7 1.5 convolution_convert_fusion.13
  82.3 0.8 pad_maximum_fusion.1
  83.1 1.6 convolution_convert_fusion.14
  84.8 1.7 convolution_convert_fusion.15
  86.5 0.6 collective-permute-start.3
  87.0 0.7 select_reduce_fusion
  88.0 2.5 %fusion.22 = f32[320,256]{1,0:T(8,128)} fusion(bf16[320,2048]{1,0:T(8,128)(2,1)} %collective-permute-done.6, bf16[1,2048,256]{2,1,0:T(8,128)(2,1)S(1)} %copy-done.11), kind=kOutput, calls=%fused_computation.47 | convolution fusion | flops 335544320 | bytes 2686976 | tf_op jit(solution)/shard_map/dot_general | solution.py:253
  90.6 4.4 %convolution_convert_fusion.1 = bf16[320,2048]{1,0:T(8,128)(2,1)} fusion(bf16[1,256,2048]{2,1,0:T(8,128)(2,1)S(1)} %copy-done, f32[320,256]{1,0:T(8,128)} %fusion.22, bf16[320,2048]{1,0:T(8,128)(2,1)} %collective-permute-done.6, bf16[1,2048,256]{2,1,0:T(8,128)(2,1)} %param.34), kind=kOutput, calls=%fused_computation.1 | convolution fusion | flops 672235520 | bytes 5046272 | tf_op jit(solution)/shard_map/dot_general | solution.py:255
  95.1 1.5 fusion.5
  96.6 0.5 collective-permute-start.12
  97.1 2.9 %fusion.26 = f32[320,256]{1,0:T(8,128)} fusion(bf16[320,2048]{1,0:T(8,128)(2,1)} %collective-permute-done.3, bf16[1,2048,256]{2,1,0:T(8,128)(2,1)} %param.35), kind=kOutput, calls=%fused_computation.51 | convolution fusion | flops 335544320 | bytes 2686976 | tf_op jit(solution)/shard_map/dot_general | solution.py:253
  100.0 4.4 %convolution_convert_fusion.3 = bf16[320,2048]{1,0:T(8,128)(2,1)} fusion(bf16[1,256,2048]{2,1,0:T(8,128)(2,1)S(1)} %copy-done, f32[320,256]{1,0:T(8,128)} %fusion.26, bf16[320,2048]{1,0:T(8,128)(2,1)} %collective-permute-done.3, bf16[1,2048,256]{2,1,0:T(8,128)(2,1)} %param.34), kind=kOutput, calls=%fused_computation.4 | convolution fusion | flops 672235520 | bytes 5046272 | tf_op jit(solution)/shard_map/dot_general | solution.py:255
  104.3 2.8 %fusion.24 = f32[320,256]{1,0:T(8,128)} fusion(bf16[320,2048]{1,0:T(8,128)(2,1)} %collective-permute-done.5, bf16[1,2048,256]{2,1,0:T(8,128)(2,1)} %param.35), kind=kOutput, calls=%fused_computation.49 | convolution fusion | flops 335544320 | bytes 2686976 | tf_op jit(solution)/shard_map/dot_general | solution.py:253
  107.2 4.8 %add_convert_fusion.1 = bf16[320,2048]{1,0:T(8,128)(2,1)} fusion(bf16[320,2048]{1,0:T(8,128)(2,1)} %collective-permute-done.7, bf16[1,256,2048]{2,1,0:T(8,128)(2,1)S(1)} %copy-done, f32[320,256]{1,0:T(8,128)} %fusion.24, bf16[320,2048]{1,0:T(8,128)(2,1)} %collective-permute-done.5, bf16[1,2048,256]{2,1,0:T(8,128)(2,1)} %param.34), kind=kOutput, calls=%fused_computation.10 | convolution fusion | flops 674856960 | bytes 6356992 | tf_op jit(solution)/shard_map/dot_general | solution.py:255
  111.9 0.5 collective-permute-start.8
  112.4 1.3 fusion.106
  113.8 2.4 %convolution_convert_fusion.7 = bf16[128,2048]{1,0:T(8,128)(2,1)} fusion(bf16[128,2048]{1,0:T(8,128)(2,1)S(1)} %copy-done.6, f32[128,128]{1,0:T(8,128)S(1)} %fusion.106, bf16[128,2048]{1,0:T(8,128)(2,1)} %collective-permute-done.9, bf16[2048,128]{1,0:T(8,128)(2,1)S(1)} %copy-done.7), kind=kOutput, calls=%fused_computation.17 | convolution fusion | flops 134578176 | bytes 2162688 | tf_op jit(solution)/shard_map/dot_general | solution.py:246
  116.4 1.3 fusion.108
  117.7 2.1 fusion.36
  119.9 4.7 %fusion.1 = f32[320,2048]{1,0:T(8,128)} fusion(bf16[320,2048]{1,0:T(8,128)(2,1)} %bitcast.5, bf16[1,256,2048]{2,1,0:T(8,128)(2,1)S(1)} %copy-done, bf16[1,2048,256]{2,1,0:T(8,128)(2,1)} %param.35, f32[320,256]{1,0:T(8,128)S(1)} %fusion.36), kind=kOutput, calls=%fused_computation.6 | convolution fusion | flops 672890880 | bytes 6356992 | tf_op jit(solution)/shard_map/dot_general | solution.py:255
  124.5 18.9 %collective-permute-done.8 = bf16[320,2048]{1,0:T(8,128)(2,1)} collective-permute-done((bf16[320,2048]{1,0:T(8,128)(2,1)}, bf16[320,2048]{1,0:T(8,128)(2,1)}, u32[]{:S(2)}, u32[]{:S(2)}) %collective-permute-start.8) | collective-permute-done | bytes 1310752 | tf_op jit(solution)/shard_map/ppermute | solution.py:124
  143.4 4.2 %add_convert_fusion = bf16[320,2048]{1,0:T(8,128)(2,1)} fusion(bf16[320,2048]{1,0:T(8,128)(2,1)} %collective-permute-done.8, f32[320,2048]{1,0:T(8,128)} %fusion.1, bf16[320,2048]{1,0:T(8,128)(2,1)} %collective-permute-done.4), kind=kLoop, calls=%fused_computation.9 | loop fusion | flops 3276800 | bytes 6553600 | tf_op jit(solution)/shard_map/convert_element_type | solution.py:270
  147.6 6.6 %all-to-all-start.1 = ((bf16[8,40,2048]{2,1,0:T(8,128)(2,1)}), bf16[8,40,2048]{2,1,0:T(8,128)(2,1)}, u32[]{:S(2)}, u32[]{:S(2)}) async-start(bf16[8,40,2048]{2,1,0:T(8,128)(2,1)} %bitcast.99), calls=%async_computation.1 | async-start | bytes 2621440 | tf_op jit(solution)/shard_map/all_to_all | solution.py:271
  154.2 2.4 %convolution_convert_fusion.5 = bf16[128,2048]{1,0:T(8,128)(2,1)} fusion(bf16[128,2048]{1,0:T(8,128)(2,1)S(1)} %copy-done.6, f32[128,128]{1,0:T(8,128)S(1)} %fusion.108, bf16[128,2048]{1,0:T(8,128)(2,1)} %collective-permute-done.12, bf16[2048,128]{1,0:T(8,128)(2,1)S(1)} %copy-done.7), kind=kOutput, calls=%fused_computation.14 | convolution fusion | flops 134578176 | bytes 2162688 | tf_op jit(solution)/shard_map/dot_general | solution.py:246
  156.6 1.3 fusion.107
  157.9 1.2 copy-done.1
  159.2 18.5 %attention.1 = bf16[256,256]{1,0:T(8,128)(2,1)S(1)} custom-call(s32[1]{0:T(128)} %bitcast.rank_ref, f32[2]{0:T(128)S(1)} %copy-done.2, bf16[256,256]{1,0:T(8,128)(2,1)S(1)} %pad_maximum_fusion.queries_ref, bf16[2048,256]{1,0:T(8,128)(2,1)S(1)} %copy-done.1, f32[1,128]{1,0:T(1,128)S(1)} %bitcast.97), custom_call_target="tpu_custom_call" | custom-call | flops 1073741824 | bytes 1048576 | tf_op jit(solution)/shard_map/attention/pallas_call | solution.py:105
  177.6 1.0 convolution_convert_fusion.9
  178.6 0.5 collective-permute-start.1
  179.2 2.5 %add_convert_fusion.2 = bf16[128,2048]{1,0:T(8,128)(2,1)} fusion(bf16[128,2048]{1,0:T(8,128)(2,1)} %collective-permute-done.13, bf16[128,2048]{1,0:T(8,128)(2,1)S(1)} %copy-done.6, f32[128,128]{1,0:T(8,128)S(1)} %fusion.107, bf16[128,2048]{1,0:T(8,128)(2,1)} %collective-permute-done.11, bf16[2048,128]{1,0:T(8,128)(2,1)S(1)} %copy-done.7), kind=kOutput, calls=%fused_computation.62 | convolution fusion | flops 135626752 | bytes 2686976 | tf_op jit(solution)/shard_map/dot_general | solution.py:246
  182.6 1.3 add_convert_fusion.4
  183.8 1.6 collective-permute-start.2
  185.8 15.6 %collective-permute-done.2 = bf16[64,2048]{1,0:T(8,128)(2,1)S(1)} collective-permute-done((bf16[64,2048]{1,0:T(8,128)(2,1)S(1)}, bf16[64,2048]{1,0:T(8,128)(2,1)S(1)}, u32[]{:S(2)}, u32[]{:S(2)}) %collective-permute-start.2) | collective-permute-done | bytes 262176 | tf_op jit(solution)/shard_map/ppermute | solution.py:124
  201.3 0.8 add_convert_fusion.3
  202.1 1.9 fusion.62
  204.0 2.9 %fusion.3 = bf16[128,2048]{1,0:T(8,128)(2,1)} fusion(f32[128,2048]{1,0:T(8,128)S(1)} %fusion.62, bf16[320,2048]{1,0:T(8,128)(2,1)} %bitcast.10, bf16[128,2048]{1,0:T(8,128)(2,1)} %collective-permute-done.14, f32[128,2048]{1,0:T(8,128)S(1)} %copy-done.8, bf16[128,2048]{1,0:T(8,128)(2,1)} %collective-permute-done.10, f32[128,320]{0,1:T(8,128)S(1)} %copy-done.10), kind=kOutput, calls=%fused_computation.13 | convolution fusion | flops 169689088 | bytes 5144576 | tf_op jit(solution)/shard_map/dot_general | solution.py:289
  (78 shorter events, 3.3 us)
Async XLA Ops:
  7.2 83.4 %copy-start = (bf16[1,256,2048]{2,1,0:T(8,128)(2,1)S(1)}, bf16[1,256,2048]{2,1,0:T(8,128)(2,1)}, u32[]{:S(2)}) copy-start(bf16[1,256,2048]{2,1,0:T(8,128)(2,1)} %param.36) | copy-start | bytes 3145732
  7.2 4.4 %copy-start.9 = (bf16[128,2048]{1,0:T(8,128)(2,1)S(1)}, bf16[128,2048]{1,0:T(8,128)(2,1)}, u32[]{:S(2)}) copy-start(bf16[128,2048]{1,0:T(8,128)(2,1)} %param.30) | copy-start | bytes 1572868
  7.2 150.7 %all-gather.2.cloned.1.call-start = ((), (), s32[]{:S(2)}) async-start(), calls=%async_computation.2 | async-start | bytes 1179648 | tf_op jit(solution)/shard_map/all_gather | solution.py:200
  13.0 37.1 %copy-start.12 = (bf16[256,2048]{1,0:T(8,128)(2,1)S(1)}, bf16[256,2048]{1,0:T(8,128)(2,1)}, u32[]{:S(2)}) copy-start(bf16[256,2048]{1,0:T(8,128)(2,1)} %param.20) | copy-start | bytes 3145732
  13.0 37.4 %copy-start.15 = (bf16[2048,64]{0,1:T(8,128)(2,1)S(1)}, bf16[2048,64]{0,1:T(8,128)(2,1)}, u32[]{:S(2)}) copy-start(bf16[2048,64]{0,1:T(8,128)(2,1)} %param.24) | copy-start | bytes 786436
  13.0 37.4 %copy-start.17 = (f32[2048]{0:T(1024)S(1)}, f32[2048]{0:T(1024)}, u32[]{:S(2)}) copy-start(f32[2048]{0:T(1024)} %param.21) | copy-start | bytes 24580
  48.0 32.0 %collective-permute-start.5 = (bf16[320,2048]{1,0:T(8,128)(2,1)}, bf16[320,2048]{1,0:T(8,128)(2,1)}, u32[]{:S(2)}, u32[]{:S(2)}) collective-permute-start(bf16[320,2048]{1,0:T(8,128)(2,1)} %bitcast.5), channel_id=1, source_target_pairs={{0,2},{1,3},{2,0},{3,1},{4,6},{5,7},{6,4},{7,5},{8,10},{9,11},{10,... | collective-permute-start | bytes 3932168 | tf_op jit(solution)/shard_map/ppermute | solution.py:124
  48.5 48.1 %collective-permute-start.11 = (bf16[128,2048]{1,0:T(8,128)(2,1)S(1)}, bf16[128,2048]{1,0:T(8,128)(2,1)}, u32[]{:S(2)}, u32[]{:S(2)}) collective-permute-start(bf16[128,2048]{1,0:T(8,128)(2,1)S(1)} %fusion.15), channel_id=1, source_target_pairs={{0,2},{1,3},{2,0},{3,1},{4,6},{5,7},{6,4},{7,5},{8,10},{9,11},{10,... | collective-permute-start | bytes 1572872 | tf_op jit(solution)/shard_map/ppermute | solution.py:124
  50.0 62.4 %collective-permute-start.9 = (bf16[128,2048]{1,0:T(8,128)(2,1)S(1)}, bf16[128,2048]{1,0:T(8,128)(2,1)}, u32[]{:S(2)}, u32[]{:S(2)}) collective-permute-start(bf16[128,2048]{1,0:T(8,128)(2,1)S(1)} %fusion.15), channel_id=1, source_target_pairs={{0,1},{1,0},{2,3},{3,2},{4,5},{5,4},{6,7},{7,6},{8,9},{9,8},{10,11... | collective-permute-start | bytes 1572872 | tf_op jit(solution)/shard_map/ppermute | solution.py:124
  50.3 29.7 %copy-start.16 = (bf16[2048,64]{0,1:T(8,128)(2,1)S(1)}, bf16[2048,64]{0,1:T(8,128)(2,1)}, u32[]{:S(2)}) copy-start(bf16[2048,64]{0,1:T(8,128)(2,1)} %param.25) | copy-start | bytes 786436
  80.0 8.0 %collective-permute-start.6 = (bf16[320,2048]{1,0:T(8,128)(2,1)}, bf16[320,2048]{1,0:T(8,128)(2,1)}, u32[]{:S(2)}, u32[]{:S(2)}) collective-permute-start(bf16[320,2048]{1,0:T(8,128)(2,1)} %collective-permute-done.5), channel_id=1, source_target_pairs={{0,1},{1,0},{2,3},{3,2},{4,5},{5,4},{6,7},{7,6},{8,9},{9,8},{10,11... | collective-permute-start | bytes 3932168 | tf_op jit(solution)/shard_map/ppermute | solution.py:124
  83.1 1.6 copy-start.13
  84.7 2.3 %copy-start.14 = (f32[128,2]{0,1:T(2,128)S(1)}, f32[128,2]{0,1:T(2,128)}, u32[]{:S(2)}) copy-start(f32[128,2]{0,1:T(2,128)} %param.33) | copy-start | bytes 3076
  84.8 3.0 %copy-start.5 = (bf16[2048,128]{1,0:T(8,128)(2,1)S(1)}, bf16[2048,128]{1,0:T(8,128)(2,1)}, u32[]{:S(2)}) copy-start(bf16[2048,128]{1,0:T(8,128)(2,1)} %param.37) | copy-start | bytes 1572868
  84.8 3.3 %copy-start.11 = (bf16[1,2048,256]{2,1,0:T(8,128)(2,1)S(1)}, bf16[1,2048,256]{2,1,0:T(8,128)(2,1)}, u32[]{:S(2)}) copy-start(bf16[1,2048,256]{2,1,0:T(8,128)(2,1)} %param.35) | copy-start | bytes 3145732
  86.5 10.7 %collective-permute-start.3 = (bf16[320,2048]{1,0:T(8,128)(2,1)}, bf16[320,2048]{1,0:T(8,128)(2,1)}, u32[]{:S(2)}, u32[]{:S(2)}) collective-permute-start(bf16[320,2048]{1,0:T(8,128)(2,1)} %bitcast.5), channel_id=1, source_target_pairs={{0,1},{1,0},{2,3},{3,2},{4,5},{5,4},{6,7},{7,6},{8,9},{9,8},{10,11... | collective-permute-start | bytes 3932168 | tf_op jit(solution)/shard_map/ppermute | solution.py:124
  90.6 4.5 %copy-start.6 = (bf16[128,2048]{1,0:T(8,128)(2,1)S(1)}, bf16[128,2048]{1,0:T(8,128)(2,1)}, u32[]{:S(2)}) copy-start(bf16[128,2048]{1,0:T(8,128)(2,1)} %param.39) | copy-start | bytes 1572868
  90.6 4.5 %copy-start.7 = (bf16[2048,128]{1,0:T(8,128)(2,1)S(1)}, bf16[2048,128]{1,0:T(8,128)(2,1)}, u32[]{:S(2)}) copy-start(bf16[2048,128]{1,0:T(8,128)(2,1)} %param.38) | copy-start | bytes 1572868
  95.0 12.1 %collective-permute-start.7 = (bf16[320,2048]{1,0:T(8,128)(2,1)}, bf16[320,2048]{1,0:T(8,128)(2,1)}, u32[]{:S(2)}, u32[]{:S(2)}) collective-permute-start(bf16[320,2048]{1,0:T(8,128)(2,1)} %convolution_convert_fusion.1), channel_id=1, source_target_pairs={{0,1},{1,0},{2,3},{3,2},{4,5},{5,4},{6,7},{7,6},{8,9},{9,8},{10,11... | collective-permute-start | bytes 3932168 | tf_op jit(solution)/shard_map/ppermute | solution.py:124
  96.6 19.8 %collective-permute-start.12 = (bf16[128,2048]{1,0:T(8,128)(2,1)}, bf16[128,2048]{1,0:T(8,128)(2,1)}, u32[]{:S(2)}, u32[]{:S(2)}) collective-permute-start(bf16[128,2048]{1,0:T(8,128)(2,1)} %collective-permute-done.11), channel_id=1, source_target_pairs={{0,1},{1,0},{2,3},{3,2},{4,5},{5,4},{6,7},{7,6},{8,9},{9,8},{10,11... | collective-permute-start | bytes 1572872 | tf_op jit(solution)/shard_map/ppermute | solution.py:124
  104.3 20.2 %collective-permute-start.4 = (bf16[320,2048]{1,0:T(8,128)(2,1)}, bf16[320,2048]{1,0:T(8,128)(2,1)}, u32[]{:S(2)}, u32[]{:S(2)}) collective-permute-start(bf16[320,2048]{1,0:T(8,128)(2,1)} %convolution_convert_fusion.3), channel_id=1, source_target_pairs={{0,1},{1,0},{2,3},{3,2},{4,5},{5,4},{6,7},{7,6},{8,9},{9,8},{10,11... | collective-permute-start | bytes 3932168 | tf_op jit(solution)/shard_map/ppermute | solution.py:124
  111.9 31.5 %collective-permute-start.8 = (bf16[320,2048]{1,0:T(8,128)(2,1)}, bf16[320,2048]{1,0:T(8,128)(2,1)}, u32[]{:S(2)}, u32[]{:S(2)}) collective-permute-start(bf16[320,2048]{1,0:T(8,128)(2,1)} %add_convert_fusion.1), channel_id=1, source_target_pairs={{0,2},{1,3},{2,0},{3,1},{4,6},{5,7},{6,4},{7,5},{8,10},{9,11},{10,... | collective-permute-start | bytes 3932168 | tf_op jit(solution)/shard_map/ppermute | solution.py:124
  116.2 87.8 %collective-permute-start.10 = (bf16[128,2048]{1,0:T(8,128)(2,1)}, bf16[128,2048]{1,0:T(8,128)(2,1)}, u32[]{:S(2)}, u32[]{:S(2)}) collective-permute-start(bf16[128,2048]{1,0:T(8,128)(2,1)} %convolution_convert_fusion.7), channel_id=1, source_target_pairs={{0,1},{1,0},{2,3},{3,2},{4,5},{5,4},{6,7},{7,6},{8,9},{9,8},{10,11... | collective-permute-start | bytes 1572872 | tf_op jit(solution)/shard_map/ppermute | solution.py:124
  147.6 54.5 %all-to-all-start.1 = ((bf16[8,40,2048]{2,1,0:T(8,128)(2,1)}), bf16[8,40,2048]{2,1,0:T(8,128)(2,1)}, u32[]{:S(2)}, u32[]{:S(2)}) async-start(bf16[8,40,2048]{2,1,0:T(8,128)(2,1)} %bitcast.99), calls=%async_computation.1 | async-start | bytes 2621440 | tf_op jit(solution)/shard_map/all_to_all | solution.py:271
  154.2 3.8 %copy-start.2 = (f32[2]{0:T(128)S(1)}, f32[2]{0:T(128)}, u32[]{:S(2)}) copy-start(f32[2]{0:T(128)} %lambdas_ref.1) | copy-start | bytes 28
  154.2 3.8 %copy-start.3 = (f32[128]{0:T(128)S(1)}, f32[128]{0:T(128)}, u32[]{:S(2)}) copy-start(f32[128]{0:T(128)} %param.28) | copy-start | bytes 1540
  156.6 22.6 %collective-permute-start.13 = (bf16[128,2048]{1,0:T(8,128)(2,1)}, bf16[128,2048]{1,0:T(8,128)(2,1)}, u32[]{:S(2)}, u32[]{:S(2)}) collective-permute-start(bf16[128,2048]{1,0:T(8,128)(2,1)} %convolution_convert_fusion.5), channel_id=1, source_target_pairs={{0,1},{1,0},{2,3},{3,2},{4,5},{5,4},{6,7},{7,6},{8,9},{9,8},{10,11... | collective-permute-start | bytes 1572872 | tf_op jit(solution)/shard_map/ppermute | solution.py:124
  157.9 1.2 copy-start.1
  159.2 18.5 %copy-start.4 = (bf16[256,2048]{1,0:T(8,128)(2,1)S(1)}, bf16[256,2048]{1,0:T(8,128)(2,1)}, u32[]{:S(2)}) copy-start(bf16[256,2048]{1,0:T(8,128)(2,1)} %param.29) | copy-start | bytes 3145732
  178.6 3.9 %collective-permute-start.1 = (bf16[64,2048]{1,0:T(8,128)(2,1)}, bf16[64,2048]{1,0:T(8,128)(2,1)}, u32[]{:S(2)}, u32[]{:S(2)}) collective-permute-start(bf16[64,2048]{1,0:T(8,128)(2,1)} %convolution_convert_fusion.9), channel_id=1, source_target_pairs={{0,1},{1,0},{2,3},{3,2},{4,5},{5,4},{6,7},{7,6},{8,9},{9,8},{10,11... | collective-permute-start | bytes 786440 | tf_op jit(solution)/shard_map/ppermute | solution.py:124
  181.7 22.3 %collective-permute-start.14 = (bf16[128,2048]{1,0:T(8,128)(2,1)}, bf16[128,2048]{1,0:T(8,128)(2,1)}, u32[]{:S(2)}, u32[]{:S(2)}) collective-permute-start(bf16[128,2048]{1,0:T(8,128)(2,1)} %add_convert_fusion.2), channel_id=1, source_target_pairs={{0,2},{1,3},{2,0},{3,1},{4,6},{5,7},{6,4},{7,5},{8,10},{9,11},{10,... | collective-permute-start | bytes 1572872 | tf_op jit(solution)/shard_map/ppermute | solution.py:124
  182.5 3.3 %collective-permute-start = (bf16[64,2048]{1,0:T(8,128)(2,1)S(1)}, bf16[64,2048]{1,0:T(8,128)(2,1)S(1)}, u32[]{:S(2)}, u32[]{:S(2)}) collective-permute-start(bf16[64,2048]{1,0:T(8,128)(2,1)S(1)} %convolution_convert_fusion.11), channel_id=1, source_target_pairs={{0,1},{1,0},{2,3},{3,2},{4,5},{5,4},{6,7},{7,6},{8,9},{9,8},{10,11... | collective-permute-start | bytes 786440 | tf_op jit(solution)/shard_map/ppermute | solution.py:124
  183.8 18.3 %copy-start.10 = (f32[128,320]{0,1:T(8,128)S(1)}, f32[128,320]{0,1:T(8,128)}, u32[]{:S(2)}) copy-start(f32[128,320]{0,1:T(8,128)} %select_reduce_fusion) | copy-start | bytes 491524
  183.8 17.5 %collective-permute-start.2 = (bf16[64,2048]{1,0:T(8,128)(2,1)S(1)}, bf16[64,2048]{1,0:T(8,128)(2,1)S(1)}, u32[]{:S(2)}, u32[]{:S(2)}) collective-permute-start(bf16[64,2048]{1,0:T(8,128)(2,1)S(1)} %add_convert_fusion.4), channel_id=1, source_target_pairs={{0,2},{1,3},{2,0},{3,1},{4,6},{5,7},{6,4},{7,5},{8,10},{9,11},{10,... | collective-permute-start | bytes 786440 | tf_op jit(solution)/shard_map/ppermute | solution.py:124
  202.1 1.9 copy-start.8
Sparse Core Ops, SparseCore 0:
  83.2 39.1 all-gather.1

commit v3 on v2

--- a/solution.py
+++ b/solution.py
@@ -124,12 +124,16 @@
     return lax.ppermute(rows, axis, [(i, i ^ distance) for i in range(size)])
 
 
-def gather_near(block, axis, size):
+def gather_near(block, axis, size, ahead=None):
     places = {0: block}
     distance = size // 2
     while distance:
         for place in sorted(places):
-            places[place ^ distance] = swap(places[place], axis, size, distance)
+            moved = swap(places[place], axis, size, distance)
+            if ahead is not None:
+                moved, ahead = lax.optimization_barrier((moved, ahead))
+            places[place ^ distance] = moved
+        ahead = None
         distance //= 2
     return [places[place] for place in range(size)]
 
@@ -234,6 +238,7 @@
     )
     pair_rows = experts_local * capacity
     outgoing = outgoing.reshape(ep_size, pair_rows, model_width)
+    outgoing, key_values = lax.optimization_barrier((outgoing, key_values))
     received = lax.all_to_all(outgoing, "ep", split_axis=0, concat_axis=0, tiled=True)
     received = received.reshape(ep_size, experts_local, capacity, model_width)
     if experts_local == 1:
@@ -263,7 +268,7 @@
         ).astype(jnp.bfloat16)
 
     shared_places = gather_near(normed_experts, "tp", tp_size)
-    routed_places = gather_near(received, "tp", tp_size)
+    routed_places = gather_near(received, "tp", tp_size, head_rows)
     shared_result = scatter_near([shared_expert(rows) for rows in shared_places], "tp", tp_size)
     routed_result = scatter_near(
         [routed_expert(rows) for rows in routed_places], "tp", tp_size

time: 215 us -> 211 us (0.981); the launches traced: 214 us -> 207 us
  blocking collectives: 35 us -> 0 us
  waiting for transfers between devices: 63.6 us -> 85.5 us
  starting transfers between devices: 13.1 us -> 17.5 us
  matrix products: 55.7 us -> 59.1 us
    all_to_all x1 -> x0, blocking collectives: 35 us -> none  [body(): lax.all_to_all(outgoing, 'ep', split_axis=0, concat_axis=0, tiled=True)]
    all_to_all x0 -> x1, waiting for transfers between devices: none -> 32.6 us  [body(): lax.all_to_all(outgoing, 'ep', split_axis=0, concat_axis=0, tiled=True)]
    ppermute x15, waiting for transfers between devices: 63.6 us -> 37.6 us  [swap(): return lax.ppermute(rows, axis, [(i, i ^ distance) for i in range(size)])]
    all_gather x1, waiting for transfers between devices: 0.02 us -> 14.5 us  [body(): arrived = lax.all_gather(key_values, 'ep', axis=0, tiled=True)]
    all_to_all x0 -> x1, starting transfers between devices: none -> 6 us  [body(): lax.all_to_all(outgoing, 'ep', split_axis=0, concat_axis=0, tiled=True)]
  transfers between devices with their start and end apart: 17 -> 18, of which waited for: 3 -> 6; matrix products, arithmetic and copies ran while one was open for 28% -> 27% of each run, Pallas kernels for 9% -> 9%
where the time goes in v3:
time: 211 us; the launch traced here: 207 us
  waiting for transfers between devices  85.5 us (41%)
  matrix products  59.1 us (28%)
  Pallas kernels  18.6 us (9%)
  starting transfers between devices  17.5 us (8%)
  between operations  14.4 us (7%)
  other arithmetic  9.13 us (4%)
  local copies, waits for them, and re-layouts  3.11 us (1%)
    ppermute x15, waiting for transfers between devices, swap(): return lax.ppermute(rows, axis, [(i, i ^ distance) for i in range(size)])  37.6 us
    all_to_all x1, waiting for transfers between devices, body(): lax.all_to_all(outgoing, 'ep', split_axis=0, concat_axis=0, tiled=True)  32.6 us
    pallas_call x1, Pallas kernels, attention(): pl.pallas_call(functools.partial(attention_kernel, (rows, chunk, local_kv...  18.6 us
    dot_general x4, matrix products, routed_expert(): jnp.dot(hidden, expert_down[0], preferred_element_type=jnp.float32)  17.9 us
    all_gather x1, waiting for transfers between devices, body(): arrived = lax.all_gather(key_values, 'ep', axis=0, tiled=True)  14.5 us
    dot_general x4, matrix products, shared_expert(): jnp.dot(hidden, shared_down, preferred_element_type=jnp.float32)  9.52 us
    dot_general x3, matrix products, routed_expert(): lifted = jnp.dot(rows, expert_up[0], preferred_element_type=jnp.float32)  8.27 us
    dot_general x5, matrix products, project(): jnp.dot(normed, weight, preferred_element_type=jnp.float32)  7.08 us
  transfers between devices with their start and end apart: 18, of which 6 were waited for; matrix products, arithmetic and copies ran while one was open for 27% of the time, Pallas kernels for 9%

profile of v3, /device:TPU:30, one launch (start us, length us, event | category | flops | bytes accessed | tf_op | source)
XLA Modules:
  0.0 207.3 jit_solution(6992863228179343315)
XLA Ops:
  7.2 0.9 copy.56
  8.3 1.5 fusion.8
  9.9 1.9 convolution_convert_fusion.17
  12.6 1.6 convolution_convert_fusion.13
  14.2 0.6 reduce-window.6
  15.8 1.6 convolution_convert_fusion
  17.4 0.8 pad_maximum_fusion.1
  18.2 6.0 %all-to-all-start = ((bf16[8,40,2048]{2,1,0:T(8,128)(2,1)}), bf16[8,40,2048]{2,1,0:T(8,128)(2,1)}, u32[]{:S(2)}, u32[]{:S(2)}) async-start(bf16[8,40,2048]{2,1,0:T(8,128)(2,1)} %bitcast.100), calls=%async_computation | async-start | bytes 2621440 | tf_op jit(solution)/shard_map/all_to_all | solution.py:242
  24.2 0.7 all-gather.2.cloned.1.call-update
  24.9 32.6 %all-to-all-done = bf16[8,40,2048]{2,1,0:T(8,128)(2,1)} async-done(((bf16[8,40,2048]{2,1,0:T(8,128)(2,1)}), bf16[8,40,2048]{2,1,0:T(8,128)(2,1)}, u32[]{:S(2)}, u32[]{:S(2)}) %all-to-all-start) | async-done | bytes 1310752 | tf_op jit(solution)/shard_map/all_to_all | solution.py:242
  57.5 0.5 collective-permute-start.5
  58.0 1.5 convolution_convert_fusion.14
  59.6 1.6 convolution_convert_fusion.15
  61.2 14.5 %all-gather.2.cloned.1.call-done.keys_ref = bf16[2048,256]{1,0:T(8,128)(2,1)} async-done(((bf16[256,256]{1,0:T(8,128)(2,1)}), bf16[2048,256]{1,0:T(8,128)(2,1)}) %all-gather.2.cloned.1.call-update) | async-done | bytes 1048592 | tf_op jit(solution)/shard_map/all_gather | solution.py:204
  75.7 1.2 copy-done.1
  77.0 18.6 %attention.1 = bf16[256,256]{1,0:T(8,128)(2,1)S(1)} custom-call(s32[1]{0:T(128)} %bitcast.rank_ref, f32[2]{0:T(128)S(1)} %copy-done.2, bf16[256,256]{1,0:T(8,128)(2,1)S(1)} %pad_maximum_fusion.queries_ref, bf16[2048,256]{1,0:T(8,128)(2,1)S(1)} %copy-done.1, f32[1,128]{1,0:T(1,128)S(1)} %bitcast.97), custom_call_target="tpu_custom_call" | custom-call | flops 1073741824 | bytes 1048576 | tf_op jit(solution)/shard_map/attention/pallas_call | solution.py:105
  96.2 0.6 collective-permute-start.11
  97.0 2.0 collective-permute-done.6
  99.1 2.6 %fusion.22 = f32[320,256]{1,0:T(8,128)} fusion(bf16[320,2048]{1,0:T(8,128)(2,1)} %collective-permute-done.6, bf16[1,2048,256]{2,1,0:T(8,128)(2,1)S(1)} %copy-done.11), kind=kOutput, calls=%fused_computation.47 | convolution fusion | flops 335544320 | bytes 2686976 | tf_op jit(solution)/shard_map/dot_general | solution.py:258
  101.6 4.4 %convolution_convert_fusion.1 = bf16[320,2048]{1,0:T(8,128)(2,1)} fusion(bf16[1,256,2048]{2,1,0:T(8,128)(2,1)S(1)} %copy-done, f32[320,256]{1,0:T(8,128)} %fusion.22, bf16[320,2048]{1,0:T(8,128)(2,1)} %collective-permute-done.6, bf16[1,2048,256]{2,1,0:T(8,128)(2,1)} %param.34), kind=kOutput, calls=%fused_computation.1 | convolution fusion | flops 672235520 | bytes 5046272 | tf_op jit(solution)/shard_map/dot_general | solution.py:260
  106.2 0.7 select_reduce_fusion
  106.9 1.5 fusion.5
  108.4 1.8 collective-permute-done.11
  110.2 2.8 %fusion.26 = f32[320,256]{1,0:T(8,128)} fusion(bf16[320,2048]{1,0:T(8,128)(2,1)} %collective-permute-done.3, bf16[1,2048,256]{2,1,0:T(8,128)(2,1)} %param.35), kind=kOutput, calls=%fused_computation.51 | convolution fusion | flops 335544320 | bytes 2686976 | tf_op jit(solution)/shard_map/dot_general | solution.py:258
  113.1 4.4 %convolution_convert_fusion.3 = bf16[320,2048]{1,0:T(8,128)(2,1)} fusion(bf16[1,256,2048]{2,1,0:T(8,128)(2,1)S(1)} %copy-done, f32[320,256]{1,0:T(8,128)} %fusion.26, bf16[320,2048]{1,0:T(8,128)(2,1)} %collective-permute-done.3, bf16[1,2048,256]{2,1,0:T(8,128)(2,1)} %param.34), kind=kOutput, calls=%fused_computation.4 | convolution fusion | flops 672235520 | bytes 5046272 | tf_op jit(solution)/shard_map/dot_general | solution.py:260
  117.4 2.8 %fusion.24 = f32[320,256]{1,0:T(8,128)} fusion(bf16[320,2048]{1,0:T(8,128)(2,1)} %collective-permute-done.5, bf16[1,2048,256]{2,1,0:T(8,128)(2,1)} %param.35), kind=kOutput, calls=%fused_computation.49 | convolution fusion | flops 335544320 | bytes 2686976 | tf_op jit(solution)/shard_map/dot_general | solution.py:258
  120.3 0.5 collective-permute-start.4
  120.8 4.8 %add_convert_fusion.1 = bf16[320,2048]{1,0:T(8,128)(2,1)} fusion(bf16[320,2048]{1,0:T(8,128)(2,1)} %collective-permute-done.7, bf16[1,256,2048]{2,1,0:T(8,128)(2,1)S(1)} %copy-done, f32[320,256]{1,0:T(8,128)} %fusion.24, bf16[320,2048]{1,0:T(8,128)(2,1)} %collective-permute-done.5, bf16[1,2048,256]{2,1,0:T(8,128)(2,1)} %param.34), kind=kOutput, calls=%fused_computation.10 | convolution fusion | flops 674856960 | bytes 6356992 | tf_op jit(solution)/shard_map/dot_general | solution.py:260
  125.5 0.5 collective-permute-start.8
  126.1 2.0 fusion.106
  128.1 1.3 fusion.108
  129.4 2.4 %convolution_convert_fusion.5 = bf16[128,2048]{1,0:T(8,128)(2,1)} fusion(bf16[128,2048]{1,0:T(8,128)(2,1)S(1)} %copy-done.6, f32[128,128]{1,0:T(8,128)S(1)} %fusion.108, bf16[128,2048]{1,0:T(8,128)(2,1)} %collective-permute-done.12, bf16[2048,128]{1,0:T(8,128)(2,1)S(1)} %copy-done.7), kind=kOutput, calls=%fused_computation.14 | convolution fusion | flops 134578176 | bytes 2162688 | tf_op jit(solution)/shard_map/dot_general | solution.py:251
  131.8 2.2 %fusion.36 = f32[320,256]{1,0:T(8,128)S(1)} fusion(bf16[320,2048]{1,0:T(8,128)(2,1)} %bitcast.5, bf16[1,2048,256]{2,1,0:T(8,128)(2,1)} %param.34), kind=kOutput, calls=%fused_computation.60 | convolution fusion | flops 335544320 | bytes 2686976 | tf_op jit(solution)/shard_map/dot_general | solution.py:257
  134.0 4.4 %fusion.1 = f32[320,2048]{1,0:T(8,128)} fusion(bf16[320,2048]{1,0:T(8,128)(2,1)} %bitcast.5, bf16[1,256,2048]{2,1,0:T(8,128)(2,1)S(1)} %copy-done, bf16[1,2048,256]{2,1,0:T(8,128)(2,1)S(1)} %copy-done.12, f32[320,256]{1,0:T(8,128)S(1)} %fusion.36), kind=kOutput, calls=%fused_computation.6 | convolution fusion | flops 672890880 | bytes 6356992 | tf_op jit(solution)/shard_map/dot_general | solution.py:260
  138.4 18.2 %collective-permute-done.8 = bf16[320,2048]{1,0:T(8,128)(2,1)} collective-permute-done((bf16[320,2048]{1,0:T(8,128)(2,1)}, bf16[320,2048]{1,0:T(8,128)(2,1)}, u32[]{:S(2)}, u32[]{:S(2)}) %collective-permute-start.8) | collective-permute-done | bytes 1310752 | tf_op jit(solution)/shard_map/ppermute | solution.py:124
  156.5 4.2 %add_convert_fusion = bf16[320,2048]{1,0:T(8,128)(2,1)} fusion(bf16[320,2048]{1,0:T(8,128)(2,1)} %collective-permute-done.8, f32[320,2048]{1,0:T(8,128)} %fusion.1, bf16[320,2048]{1,0:T(8,128)(2,1)} %collective-permute-done.4), kind=kLoop, calls=%fused_computation.9 | loop fusion | flops 3276800 | bytes 6553600 | tf_op jit(solution)/shard_map/convert_element_type | solution.py:275
  160.7 6.0 %all-to-all-start.1 = ((bf16[8,40,2048]{2,1,0:T(8,128)(2,1)}), bf16[8,40,2048]{2,1,0:T(8,128)(2,1)S(1)}, u32[]{:S(2)}, u32[]{:S(2)}) async-start(bf16[8,40,2048]{2,1,0:T(8,128)(2,1)} %bitcast.101), calls=%async_computation.1 | async-start | bytes 2621440 | tf_op jit(solution)/shard_map/all_to_all | solution.py:276
  166.7 2.8 %convolution_convert_fusion.7 = bf16[128,2048]{1,0:T(8,128)(2,1)} fusion(bf16[128,2048]{1,0:T(8,128)(2,1)} %param.39, f32[128,128]{1,0:T(8,128)} %fusion.106, bf16[128,2048]{1,0:T(8,128)(2,1)} %collective-permute-done.9, bf16[2048,128]{1,0:T(8,128)(2,1)} %param.38), kind=kOutput, calls=%fused_computation.17 | convolution fusion | flops 134578176 | bytes 2162688 | tf_op jit(solution)/shard_map/dot_general | solution.py:251
  169.5 2.1 %fusion.107 = f32[128,128]{1,0:T(8,128)} fusion(bf16[128,2048]{1,0:T(8,128)(2,1)} %collective-permute-done.11, bf16[2048,128]{1,0:T(8,128)(2,1)} %param.37), kind=kOutput, calls=%fused_computation.131 | convolution fusion | flops 67108864 | bytes 1114112 | tf_op jit(solution)/shard_map/dot_general | solution.py:248
  171.6 1.0 convolution_convert_fusion.9
  173.1 2.9 %add_convert_fusion.2 = bf16[128,2048]{1,0:T(8,128)(2,1)} fusion(bf16[128,2048]{1,0:T(8,128)(2,1)} %collective-permute-done.13, bf16[128,2048]{1,0:T(8,128)(2,1)} %param.39, f32[128,128]{1,0:T(8,128)} %fusion.107, bf16[128,2048]{1,0:T(8,128)(2,1)} %collective-permute-done.11, bf16[2048,128]{1,0:T(8,128)(2,1)} %param.38), kind=kOutput, calls=%fused_computation.62 | convolution fusion | flops 135626752 | bytes 2686976 | tf_op jit(solution)/shard_map/dot_general | solution.py:251
  176.0 0.5 collective-permute-start.14
  176.9 1.3 add_convert_fusion.4
  178.2 1.5 collective-permute-start.2
  180.0 15.6 %collective-permute-done.2 = bf16[64,2048]{1,0:T(8,128)(2,1)S(1)} collective-permute-done((bf16[64,2048]{1,0:T(8,128)(2,1)S(1)}, bf16[64,2048]{1,0:T(8,128)(2,1)S(1)}, u32[]{:S(2)}, u32[]{:S(2)}) %collective-permute-start.2) | collective-permute-done | bytes 262176 | tf_op jit(solution)/shard_map/ppermute | solution.py:124
  195.6 0.8 add_convert_fusion.3
  196.4 1.5 fusion.62
  198.0 2.5 %fusion.3 = bf16[128,2048]{1,0:T(8,128)(2,1)} fusion(f32[128,2048]{1,0:T(8,128)S(1)} %fusion.62, bf16[320,2048]{1,0:T(8,128)(2,1)S(1)} %bitcast.99, bf16[128,2048]{1,0:T(8,128)(2,1)} %collective-permute-done.14, f32[128,2048]{1,0:T(8,128)S(1)} %copy-done.8, bf16[128,2048]{1,0:T(8,128)(2,1)} %collective-permute-done.10, f32[128,320]{0,1:T(8,128)S(1)} %copy-done.10), kind=kOutput, calls=%fused_computation.13 | convolution fusion | flops 169689088 | bytes 5144576 | tf_op jit(solution)/shard_map/dot_general | solution.py:294
  (81 shorter events, 4.3 us)
Async XLA Ops:
  7.2 94.5 %copy-start = (bf16[1,256,2048]{2,1,0:T(8,128)(2,1)S(1)}, bf16[1,256,2048]{2,1,0:T(8,128)(2,1)}, u32[]{:S(2)}) copy-start(bf16[1,256,2048]{2,1,0:T(8,128)(2,1)} %param.36) | copy-start | bytes 3145732
  9.8 2.0 copy-start.13
  9.9 2.0 copy-start.17
  9.9 2.0 copy-start.18
  12.6 2.8 %copy-start.15 = (s32[128,2]{0,1:T(2,128)S(1)}, s32[128,2]{0,1:T(2,128)}, u32[]{:S(2)}) copy-start(s32[128,2]{0,1:T(2,128)} %param.32) | copy-start | bytes 3076
  12.6 2.9 %copy-start.9 = (bf16[128,2048]{1,0:T(8,128)(2,1)S(1)}, bf16[128,2048]{1,0:T(8,128)(2,1)}, u32[]{:S(2)}) copy-start(bf16[128,2048]{1,0:T(8,128)(2,1)} %param.30) | copy-start | bytes 1572868
  12.6 3.1 %copy-start.14 = (f32[2048]{0:T(1024)S(1)}, f32[2048]{0:T(1024)}, u32[]{:S(2)}) copy-start(f32[2048]{0:T(1024)} %param.31) | copy-start | bytes 24580
  18.2 39.3 %all-to-all-start = ((bf16[8,40,2048]{2,1,0:T(8,128)(2,1)}), bf16[8,40,2048]{2,1,0:T(8,128)(2,1)}, u32[]{:S(2)}, u32[]{:S(2)}) async-start(bf16[8,40,2048]{2,1,0:T(8,128)(2,1)} %bitcast.100), calls=%async_computation | async-start | bytes 2621440 | tf_op jit(solution)/shard_map/all_to_all | solution.py:242
  24.2 51.6 %all-gather.2.cloned.1.call-start = ((), (), s32[]{:S(2)}) async-start(), calls=%async_computation.2 | async-start | bytes 1179648 | tf_op jit(solution)/shard_map/all_gather | solution.py:204
  57.5 38.1 %collective-permute-start.5 = (bf16[320,2048]{1,0:T(8,128)(2,1)}, bf16[320,2048]{1,0:T(8,128)(2,1)}, u32[]{:S(2)}, u32[]{:S(2)}) collective-permute-start(bf16[320,2048]{1,0:T(8,128)(2,1)} %bitcast.5), channel_id=1, source_target_pairs={{0,2},{1,3},{2,0},{3,1},{4,6},{5,7},{6,4},{7,5},{8,10},{9,11},{10,... | collective-permute-start | bytes 3932168 | tf_op jit(solution)/shard_map/ppermute | solution.py:124
  59.6 16.2 %copy-start.2 = (f32[2]{0:T(128)S(1)}, f32[2]{0:T(128)}, u32[]{:S(2)}) copy-start(f32[2]{0:T(128)} %lambdas_ref.1) | copy-start | bytes 28
  59.6 16.1 %copy-start.3 = (f32[128]{0:T(128)S(1)}, f32[128]{0:T(128)}, u32[]{:S(2)}) copy-start(f32[128]{0:T(128)} %param.28) | copy-start | bytes 1540
  75.7 1.2 copy-start.1
  77.0 19.8 %copy-start.5 = (bf16[2048,128]{1,0:T(8,128)(2,1)S(1)}, bf16[2048,128]{1,0:T(8,128)(2,1)}, u32[]{:S(2)}) copy-start(bf16[2048,128]{1,0:T(8,128)(2,1)} %param.37) | copy-start | bytes 1572868
  77.0 22.1 %copy-start.11 = (bf16[1,2048,256]{2,1,0:T(8,128)(2,1)S(1)}, bf16[1,2048,256]{2,1,0:T(8,128)(2,1)}, u32[]{:S(2)}) copy-start(bf16[1,2048,256]{2,1,0:T(8,128)(2,1)} %param.35) | copy-start | bytes 3145732
  95.6 3.4 %collective-permute-start.6 = (bf16[320,2048]{1,0:T(8,128)(2,1)}, bf16[320,2048]{1,0:T(8,128)(2,1)}, u32[]{:S(2)}, u32[]{:S(2)}) collective-permute-start(bf16[320,2048]{1,0:T(8,128)(2,1)} %collective-permute-done.5), channel_id=1, source_target_pairs={{0,1},{1,0},{2,3},{3,2},{4,5},{5,4},{6,7},{7,6},{8,9},{9,8},{10,11... | collective-permute-start | bytes 3932168 | tf_op jit(solution)/shard_map/ppermute | solution.py:124
  95.7 14.5 %collective-permute-start.3 = (bf16[320,2048]{1,0:T(8,128)(2,1)}, bf16[320,2048]{1,0:T(8,128)(2,1)}, u32[]{:S(2)}, u32[]{:S(2)}) collective-permute-start(bf16[320,2048]{1,0:T(8,128)(2,1)} %bitcast.5), channel_id=1, source_target_pairs={{0,1},{1,0},{2,3},{3,2},{4,5},{5,4},{6,7},{7,6},{8,9},{9,8},{10,11... | collective-permute-start | bytes 3932168 | tf_op jit(solution)/shard_map/ppermute | solution.py:124
  96.2 14.0 %collective-permute-start.11 = (bf16[128,2048]{1,0:T(8,128)(2,1)S(1)}, bf16[128,2048]{1,0:T(8,128)(2,1)}, u32[]{:S(2)}, u32[]{:S(2)}) collective-permute-start(bf16[128,2048]{1,0:T(8,128)(2,1)S(1)} %fusion.15), channel_id=1, source_target_pairs={{0,2},{1,3},{2,0},{3,1},{4,6},{5,7},{6,4},{7,5},{8,10},{9,11},{10,... | collective-permute-start | bytes 1572872 | tf_op jit(solution)/shard_map/ppermute | solution.py:124
  96.7 29.3 %collective-permute-start.9 = (bf16[128,2048]{1,0:T(8,128)(2,1)S(1)}, bf16[128,2048]{1,0:T(8,128)(2,1)}, u32[]{:S(2)}, u32[]{:S(2)}) collective-permute-start(bf16[128,2048]{1,0:T(8,128)(2,1)S(1)} %fusion.15), channel_id=1, source_target_pairs={{0,1},{1,0},{2,3},{3,2},{4,5},{5,4},{6,7},{7,6},{8,9},{9,8},{10,11... | collective-permute-start | bytes 1572872 | tf_op jit(solution)/shard_map/ppermute | solution.py:124
  101.6 4.6 %copy-start.16 = (f32[128,2]{0,1:T(2,128)S(1)}, f32[128,2]{0,1:T(2,128)}, u32[]{:S(2)}) copy-start(f32[128,2]{0,1:T(2,128)} %param.33) | copy-start | bytes 3076
  101.6 5.3 %copy-start.6 = (bf16[128,2048]{1,0:T(8,128)(2,1)S(1)}, bf16[128,2048]{1,0:T(8,128)(2,1)}, u32[]{:S(2)}) copy-start(bf16[128,2048]{1,0:T(8,128)(2,1)} %param.39) | copy-start | bytes 1572868
  101.6 5.3 %copy-start.7 = (bf16[2048,128]{1,0:T(8,128)(2,1)S(1)}, bf16[2048,128]{1,0:T(8,128)(2,1)}, u32[]{:S(2)}) copy-start(bf16[2048,128]{1,0:T(8,128)(2,1)} %param.38) | copy-start | bytes 1572868
  106.0 14.7 %collective-permute-start.7 = (bf16[320,2048]{1,0:T(8,128)(2,1)}, bf16[320,2048]{1,0:T(8,128)(2,1)}, u32[]{:S(2)}, u32[]{:S(2)}) collective-permute-start(bf16[320,2048]{1,0:T(8,128)(2,1)} %convolution_convert_fusion.1), channel_id=1, source_target_pairs={{0,1},{1,0},{2,3},{3,2},{4,5},{5,4},{6,7},{7,6},{8,9},{9,8},{10,11... | collective-permute-start | bytes 3932168 | tf_op jit(solution)/shard_map/ppermute | solution.py:124
  110.2 17.9 %collective-permute-start.12 = (bf16[128,2048]{1,0:T(8,128)(2,1)}, bf16[128,2048]{1,0:T(8,128)(2,1)}, u32[]{:S(2)}, u32[]{:S(2)}) collective-permute-start(bf16[128,2048]{1,0:T(8,128)(2,1)} %collective-permute-done.11), channel_id=1, source_target_pairs={{0,1},{1,0},{2,3},{3,2},{4,5},{5,4},{6,7},{7,6},{8,9},{9,8},{10,11... | collective-permute-start | bytes 1572872 | tf_op jit(solution)/shard_map/ppermute | solution.py:124
  120.3 18.1 %collective-permute-start.4 = (bf16[320,2048]{1,0:T(8,128)(2,1)}, bf16[320,2048]{1,0:T(8,128)(2,1)}, u32[]{:S(2)}, u32[]{:S(2)}) collective-permute-start(bf16[320,2048]{1,0:T(8,128)(2,1)} %convolution_convert_fusion.3), channel_id=1, source_target_pairs={{0,1},{1,0},{2,3},{3,2},{4,5},{5,4},{6,7},{7,6},{8,9},{9,8},{10,11... | collective-permute-start | bytes 3932168 | tf_op jit(solution)/shard_map/ppermute | solution.py:124
  125.5 31.0 %collective-permute-start.8 = (bf16[320,2048]{1,0:T(8,128)(2,1)}, bf16[320,2048]{1,0:T(8,128)(2,1)}, u32[]{:S(2)}, u32[]{:S(2)}) collective-permute-start(bf16[320,2048]{1,0:T(8,128)(2,1)} %add_convert_fusion.1), channel_id=1, source_target_pairs={{0,2},{1,3},{2,0},{3,1},{4,6},{5,7},{6,4},{7,5},{8,10},{9,11},{10,... | collective-permute-start | bytes 3932168 | tf_op jit(solution)/shard_map/ppermute | solution.py:124
  131.8 2.2 %copy-start.12 = (bf16[1,2048,256]{2,1,0:T(8,128)(2,1)S(1)}, bf16[1,2048,256]{2,1,0:T(8,128)(2,1)}, u32[]{:S(2)}) copy-start(bf16[1,2048,256]{2,1,0:T(8,128)(2,1)} %param.35) | copy-start | bytes 3145732
  131.8 41.3 %collective-permute-start.13 = (bf16[128,2048]{1,0:T(8,128)(2,1)}, bf16[128,2048]{1,0:T(8,128)(2,1)}, u32[]{:S(2)}, u32[]{:S(2)}) collective-permute-start(bf16[128,2048]{1,0:T(8,128)(2,1)} %convolution_convert_fusion.5), channel_id=1, source_target_pairs={{0,1},{1,0},{2,3},{3,2},{4,5},{5,4},{6,7},{7,6},{8,9},{9,8},{10,11... | collective-permute-start | bytes 1572872 | tf_op jit(solution)/shard_map/ppermute | solution.py:124
  160.7 35.7 %all-to-all-start.1 = ((bf16[8,40,2048]{2,1,0:T(8,128)(2,1)}), bf16[8,40,2048]{2,1,0:T(8,128)(2,1)S(1)}, u32[]{:S(2)}, u32[]{:S(2)}) async-start(bf16[8,40,2048]{2,1,0:T(8,128)(2,1)} %bitcast.101), calls=%async_computation.1 | async-start | bytes 2621440 | tf_op jit(solution)/shard_map/all_to_all | solution.py:276
  166.7 4.9 %copy-start.4 = (bf16[256,2048]{1,0:T(8,128)(2,1)S(1)}, bf16[256,2048]{1,0:T(8,128)(2,1)}, u32[]{:S(2)}) copy-start(bf16[256,2048]{1,0:T(8,128)(2,1)} %param.29) | copy-start | bytes 3145732
  169.5 28.4 %collective-permute-start.10 = (bf16[128,2048]{1,0:T(8,128)(2,1)}, bf16[128,2048]{1,0:T(8,128)(2,1)}, u32[]{:S(2)}, u32[]{:S(2)}) collective-permute-start(bf16[128,2048]{1,0:T(8,128)(2,1)} %convolution_convert_fusion.7), channel_id=1, source_target_pairs={{0,1},{1,0},{2,3},{3,2},{4,5},{5,4},{6,7},{7,6},{8,9},{9,8},{10,11... | collective-permute-start | bytes 1572872 | tf_op jit(solution)/shard_map/ppermute | solution.py:124
  172.6 4.3 %collective-permute-start.1 = (bf16[64,2048]{1,0:T(8,128)(2,1)}, bf16[64,2048]{1,0:T(8,128)(2,1)}, u32[]{:S(2)}, u32[]{:S(2)}) collective-permute-start(bf16[64,2048]{1,0:T(8,128)(2,1)} %convolution_convert_fusion.9), channel_id=1, source_target_pairs={{0,1},{1,0},{2,3},{3,2},{4,5},{5,4},{6,7},{7,6},{8,9},{9,8},{10,11... | collective-permute-start | bytes 786440 | tf_op jit(solution)/shard_map/ppermute | solution.py:124
  176.0 21.9 %collective-permute-start.14 = (bf16[128,2048]{1,0:T(8,128)(2,1)}, bf16[128,2048]{1,0:T(8,128)(2,1)}, u32[]{:S(2)}, u32[]{:S(2)}) collective-permute-start(bf16[128,2048]{1,0:T(8,128)(2,1)} %add_convert_fusion.2), channel_id=1, source_target_pairs={{0,2},{1,3},{2,0},{3,1},{4,6},{5,7},{6,4},{7,5},{8,10},{9,11},{10,... | collective-permute-start | bytes 1572872 | tf_op jit(solution)/shard_map/ppermute | solution.py:124
  176.8 3.2 %collective-permute-start = (bf16[64,2048]{1,0:T(8,128)(2,1)S(1)}, bf16[64,2048]{1,0:T(8,128)(2,1)S(1)}, u32[]{:S(2)}, u32[]{:S(2)}) collective-permute-start(bf16[64,2048]{1,0:T(8,128)(2,1)S(1)} %convolution_convert_fusion.11), channel_id=1, source_target_pairs={{0,1},{1,0},{2,3},{3,2},{4,5},{5,4},{6,7},{7,6},{8,9},{9,8},{10,11... | collective-permute-start | bytes 786440 | tf_op jit(solution)/shard_map/ppermute | solution.py:124
  178.2 17.4 %collective-permute-start.2 = (bf16[64,2048]{1,0:T(8,128)(2,1)S(1)}, bf16[64,2048]{1,0:T(8,128)(2,1)S(1)}, u32[]{:S(2)}, u32[]{:S(2)}) collective-permute-start(bf16[64,2048]{1,0:T(8,128)(2,1)S(1)} %add_convert_fusion.4), channel_id=1, source_target_pairs={{0,2},{1,3},{2,0},{3,1},{4,6},{5,7},{6,4},{7,5},{8,10},{9,11},{10,... | collective-permute-start | bytes 786440 | tf_op jit(solution)/shard_map/ppermute | solution.py:124
  196.4 1.5 copy-start.8
  196.4 1.5 copy-start.10
Sparse Core Ops, SparseCore 0:
  27.7 48.0 all-gather.1
